TPU v7x, 256 devices: a whole 4x4x8 slice. The times are simulated.
256 devices in a mesh: rep: 2 (over z_hi), fs: 16 (over z_lo, x), tp: 8 (over y, core).
Axes of the slice: x: 4, y: 4, z: 8 (z_hi: 2, z_lo: 4; z = z_hi * 4 + z_lo), core: 2. Of those that a mesh axis runs over, the one named last changes fastest.
Arguments:
- tokens: bfloat16 [32768, 2048], P(('rep', 'fs', 'tp')), may hold values from -6 to 6
- mix_gain: bfloat16 [2048], replicated, may hold values from 0.099609375 to 1.8984375
- gate_proj: bfloat16 [2048, 512], P('fs', 'tp'), may hold values from -0.125 to 0.125
- value_proj: bfloat16 [2048, 512], P('fs', 'tp'), may hold values from -1 to 1
- layer_gain: bfloat16 [512], replicated, may hold values from 0.099609375 to 1.8984375
- layer_shift: bfloat16 [512], replicated, may hold values from -3 to 3
- mix_kernel: bfloat16 [4, 128, 128], replicated, may hold values from -0.5 to 0.5
- mix_offset: bfloat16 [4, 128], replicated, may hold values from -4 to 4
- out_proj: bfloat16 [2048, 512], P('fs', 'tp'), may hold values from -0.25 to 0.25
- ffn_gain: bfloat16 [2048], replicated, may hold values from 0.099609375 to 1.8984375
- ffn_gate: bfloat16 [2048, 5632], P('fs', 'tp'), may hold values from -0.125 to 0.125
- ffn_up: bfloat16 [2048, 5632], P('fs', 'tp'), may hold values from -0.125 to 0.125
- ffn_down: bfloat16 [2048, 5632], P('fs', 'tp'), may hold values from -0.078125 to 0.078125
Outputs:
- layer_out: bfloat16 [32768, 2048], P(('rep', 'fs', 'tp'))
All inputs are finite; a program needn't handle non-finite values.
Results may differ from a plain program's by a relative error of at most 0.015.
Values may be sent and summed in bfloat16 or wider, within the bound.
A program may use at most 64 MiB of HBM per device.

v0:
```python
import jax
import jax.numpy as jnp
from jax import lax
from jax.sharding import Mesh
from jax.sharding import PartitionSpec as P

FS = ("fs_0", "fs_1")
TP = ("tp_0", "tp_1")
REP_FS_TP = ("rep", "fs_0", "fs_1", "tp_0", "tp_1")


epsilon = 1e-06


def side_by_side(arrays, axis, dim, along):
    widths = [a.shape[along] for a in arrays]
    both = jnp.concatenate(arrays, axis=along)
    out = lax.all_gather(both, axis, axis=dim, tiled=True)
    return tuple(jnp.split(out, [sum(widths[:k]) for k in range(1, len(widths))], axis=along))


def sent_to_all(value, axis):
    count = lax.axis_size(axis)
    return lax.all_to_all(
        jnp.broadcast_to(value[None], (count, *value.shape)), axis, 0, 0, tiled=True
    )


def in_order(blocks, dim):
    blocks = jnp.moveaxis(blocks, 0, dim)
    lengths = blocks.shape
    return blocks.reshape(*lengths[:dim], lengths[dim] * lengths[dim + 1], *lengths[dim + 2 :])


def gathered_by_axis(value, axes, dim):
    far, near = axes
    blocks = sent_to_all(sent_to_all(value, far), near)
    return in_order(blocks.swapaxes(0, 1).reshape(-1, *value.shape), dim)


def over_copies(value, axis):
    return sent_to_all(value, axis).sum(axis=0)


def in_one(arrays, axis):
    line, at, gathered = (jnp.concatenate([a.reshape(-1) for a in arrays]), 0, [])
    so_far = over_copies(line, axis)
    for a in arrays:
        gathered.append(so_far[at : at + a.size].reshape(a.shape))
        at += a.size
    return tuple(gathered)


def split_up(value, dim, count):
    lengths = value.shape
    blocks = value.reshape(*lengths[:dim], count, lengths[dim] // count, *lengths[dim + 1 :])
    return jnp.moveaxis(blocks, dim, 0)


def summed_on_arrival(value, axis, dim):
    count = lax.axis_size(axis)
    blocks = lax.all_to_all(split_up(value, dim, count), axis, 0, 0, tiled=True)
    return jnp.sum(blocks.astype(jnp.float32), axis=0)


def summed_rows(value, axes, dim):
    far, near = axes
    own = summed_on_arrival(split_up(value, dim, lax.axis_size(far)), near, dim + 1)
    return jnp.sum(
        lax.all_to_all(own.astype(jnp.bfloat16), far, 0, 0, tiled=True).astype(jnp.float32), axis=0
    )


def gather_in_order(value, axes, turns):
    blocks = value
    for k in turns:
        blocks = lax.all_gather(blocks, axes[k])
    done = turns[::-1]
    back = [done.index(k) for k in range(len(axes))]
    blocks = blocks.transpose(*back, *range(len(axes), blocks.ndim))
    return blocks.reshape(-1, *value.shape)


def whole_of(value, axes, turns, dim):
    return in_order(gather_in_order(value, axes, turns), dim)


def rms_norm(rows, gain):
    floats = rows.astype(jnp.float32)
    scale = lax.rsqrt(jnp.mean(floats * floats, axis=-1, keepdims=True) + epsilon)
    return (floats * scale * gain.astype(jnp.float32)).astype(jnp.bfloat16)


def contract_last(left, right):
    return lax.dot_general(
        left, right, (((1,), (1,)), ((), ())), preferred_element_type=jnp.float32
    )


def per_device(
    tokens,
    mix_gain,
    gate_proj,
    value_proj,
    layer_gain,
    layer_shift,
    mix_kernel,
    mix_offset,
    out_proj,
    ffn_gain,
    ffn_gate,
    ffn_up,
    ffn_down,
):
    normed = rms_norm(tokens, mix_gain)
    gate_rows, value_rows, out_rows = side_by_side((gate_proj, value_proj, out_proj), FS, 0, 1)
    mix_width = layer_gain.shape[0]
    groups = mix_kernel.shape[0]
    span_len = mix_kernel.shape[1]
    causal = jnp.tril(jnp.ones((span_len, span_len), dtype=bool))
    masked = jnp.where(causal[None], mix_kernel, jnp.zeros_like(mix_kernel))
    local_width = gate_rows.shape[1]
    first_col = lax.axis_index(TP) * local_width
    joined = jnp.concatenate([gate_rows, value_rows], axis=1)
    preact = jnp.dot(
        gathered_by_axis(normed, ("tp_0", "tp_1"), 0), joined, preferred_element_type=jnp.float32
    )
    gate_u = jax.nn.gelu(preact[:, :local_width])
    activated = jax.nn.gelu(preact[:, local_width:])
    row_sum, squares = in_one(
        (jnp.sum(activated, axis=-1), jnp.sum(activated * activated, axis=-1)), TP
    )
    center = (row_sum / mix_width)[:, None]
    spread = (squares / mix_width)[:, None] - center * center
    gain_part = lax.dynamic_slice_in_dim(layer_gain, first_col, local_width).astype(jnp.float32)
    shift_part = lax.dynamic_slice_in_dim(layer_shift, first_col, local_width).astype(jnp.float32)
    values = ((activated - center) * lax.rsqrt(spread + epsilon) * gain_part + shift_part).astype(
        jnp.bfloat16
    )
    group_id = first_col // (mix_width // groups)
    kernel = lax.dynamic_index_in_dim(masked, group_id, 0, keepdims=False)
    offset = lax.dynamic_index_in_dim(mix_offset, group_id, 0, keepdims=False).astype(jnp.float32)
    mixing = jnp.einsum(
        "ts,nsc->ntc",
        kernel,
        values.reshape(-1, span_len, local_width),
        preferred_element_type=jnp.float32,
    )
    mixing = mixing + offset[None, :, None]
    gated_rows = (gate_u * mixing.reshape(gate_u.shape)).astype(jnp.bfloat16)
    mixer_out = summed_rows(
        contract_last(gated_rows, out_rows).astype(jnp.bfloat16), ("tp_0", "tp_1"), 0
    )
    middle = (tokens.astype(jnp.float32) + mixer_out).astype(jnp.bfloat16)
    normed2 = rms_norm(middle, ffn_gain)
    gathered = gathered_by_axis(normed2, ("tp_0", "tp_1"), 0)
    pieces = side_by_side((ffn_gate, ffn_up), FS, 0, 1)
    gate_pre = jnp.dot(gathered, pieces[0], preferred_element_type=jnp.float32)
    up_pre = jnp.dot(gathered, pieces[1], preferred_element_type=jnp.float32)
    hidden = (jax.nn.silu(gate_pre) * up_pre).astype(jnp.bfloat16)
    partial_value = contract_last(hidden, whole_of(ffn_down, FS, (0, 1), 0))
    summed = summed_rows(partial_value.astype(jnp.bfloat16), ("tp_0", "tp_1"), 0)
    return (middle.astype(jnp.float32) + summed).astype(jnp.bfloat16)


def solution(mesh):
    torus = Mesh(
        mesh.devices.reshape(mesh.shape["rep"], 4, 4, 4, 2), ("rep", "fs_0", "fs_1", "tp_0", "tp_1")
    )
    return jax.shard_map(
        per_device,
        mesh=torus,
        in_specs=(
            P(REP_FS_TP, None),
            P(),
            P(FS, TP),
            P(FS, TP),
            P(),
            P(),
            P(),
            P(),
            P(FS, TP),
            P(),
            P(FS, TP),
            P(FS, TP),
            P(FS, TP),
        ),
        out_specs=P(REP_FS_TP, None),
        check_vma=False,
    )
```

profile of v0, /device:TPU:1, one launch (start us, length us, event | category | flops | bytes accessed | tf_op | source)
XLA Modules:
  0.0 264.5 jit_solution(6864890175165852455)
XLA Ops:
  6.5 17.9 %all-gather = bf16[512,704]{0,1:T(8,128)(2,1)S(1)} all-gather(bf16[128,704]{0,1:T(8,128)(2,1)} %param.25), channel_id=2, replica_groups=mesh['rep'=2,'fs_0'=4,'fs_1'=4,'tp_0'=4,'tp_1'=2] {'fs_0'}, dimensions={0}, use_global_device_ids=true | all-gather | bytes 901120 | tf_op jit(solution)/shard_map/all_gather | solution.py:77
  25.5 1.8 pad_maximum_fusion
  30.0 4.2 %all-to-all-start = ((bf16[4,128,2048]{2,1,0:T(8,128)(2,1)}), bf16[4,128,2048]{2,1,0:T(8,128)(2,1)S(1)}, u32[]{:S(2)}, u32[]{:S(2)}) async-start(bf16[4,128,2048]{2,1,0:T(8,128)(2,1)} %broadcast_in_dim.22), calls=%async_computation | async-start | bytes 4194304 | tf_op jit(solution)/shard_map/all_to_all | solution.py:24
  34.3 39.3 %all_gather.18 = bf16[2048,192]{0,1:T(8,128)(2,1)S(1)} all-gather(bf16[128,192]{0,1:T(8,128)(2,1)S(1)} %pad_maximum_fusion.1), channel_id=1, replica_groups=mesh['rep'=2,'fs_0'=4,'fs_1'=4,'tp_0'=4,'tp_1'=2] {'fs_0','fs_1'}, dimensions={0}, use_global_device_ids=true | all-gather | bytes 835584 | tf_op jit(solution)/shard_map/all_gather | solution.py:18
  74.1 15.5 %all_to_all.46 = bf16[2,4,128,2048]{3,2,1,0:T(8,128)(2,1)S(1)} all-to-all(bf16[2,4,128,2048]{3,2,1,0:T(8,128)(2,1)S(1)} %broadcast_in_dim.23), channel_id=1, replica_groups=mesh['rep'=2,'fs_0'=4,'fs_1'=4,'tp_0'=4,'tp_1'=2] {'tp_1'}, dimensions={0} | all-to-all | bytes 8388608 | tf_op jit(solution)/shard_map/all_to_all | solution.py:24
  92.5 5.4 %all-to-all-start.2 = ((f32[8,1,2048]{2,1,0:T(1,128)}), f32[8,1,2048]{2,1,0:T(1,128)S(1)}, u32[]{:S(2)}, u32[]{:S(2)}) async-start(f32[8,1,2048]{2,1,0:T(1,128)} %broadcast_in_dim.24), calls=%async_computation.2 | async-start | bytes 131072 | tf_op jit(solution)/shard_map/all_to_all | solution.py:24
  97.9 5.2 %all-to-all-done.2 = f32[8,1,2048]{2,1,0:T(1,128)S(1)} async-done(((f32[8,1,2048]{2,1,0:T(1,128)}), f32[8,1,2048]{2,1,0:T(1,128)S(1)}, u32[]{:S(2)}, u32[]{:S(2)}) %all-to-all-start.2) | async-done | bytes 65568 | tf_op jit(solution)/shard_map/all_to_all | solution.py:24
  106.1 8.1 %all_to_all.47 = bf16[2,4,128,2048]{3,2,1,0:T(8,128)(2,1)} all-to-all(bf16[2,4,128,2048]{3,2,1,0:T(8,128)(2,1)S(1)} %bitcast.49), channel_id=1, replica_groups=mesh['rep'=2,'fs_0'=4,'fs_1'=4,'tp_0'=4,'tp_1'=2] {'tp_1'}, dimensions={0} | all-to-all | bytes 8388608 | tf_op jit(solution)/shard_map/all_to_all | solution.py:62
  114.2 5.1 %reduce_sum.91 = bf16[4,128,2048]{2,1,0:T(8,128)(2,1)} reduce(bf16[2,4,128,2048]{3,2,1,0:T(8,128)(2,1)} %all_to_all.47, bf16[]{:T(256)} %constant.64.clone.1), dimensions={0}, to_apply=%region_4.5 | reduce | flops 1048576 | bytes 6291458 | tf_op jit(solution)/shard_map/reduce_sum | solution.py:63
  119.4 3.6 %all-to-all-start.4 = ((bf16[4,128,2048]{2,1,0:T(8,128)(2,1)}), bf16[4,128,2048]{2,1,0:T(8,128)(2,1)S(1)}, u32[]{:S(2)}, u32[]{:S(2)}) async-start(bf16[4,128,2048]{2,1,0:T(8,128)(2,1)} %reduce_sum.91), calls=%async_computation.4 | async-start | bytes 4194304 | tf_op jit(solution)/shard_map/all_to_all | solution.py:70
  123.0 26.0 %all-to-all-done.4 = bf16[4,128,2048]{2,1,0:T(8,128)(2,1)S(1)} async-done(((bf16[4,128,2048]{2,1,0:T(8,128)(2,1)}), bf16[4,128,2048]{2,1,0:T(8,128)(2,1)S(1)}, u32[]{:S(2)}, u32[]{:S(2)}) %all-to-all-start.4) | async-done | bytes 2097184 | tf_op jit(solution)/shard_map/all_to_all | solution.py:70
  151.5 4.5 %all-to-all-start.5 = ((bf16[4,128,2048]{2,1,0:T(8,128)(2,1)}), bf16[4,128,2048]{2,1,0:T(8,128)(2,1)}, u32[]{:S(2)}, u32[]{:S(2)}) async-start(bf16[4,128,2048]{2,1,0:T(8,128)(2,1)} %broadcast_in_dim.27), calls=%async_computation.5 | async-start | bytes 4194304 | tf_op jit(solution)/shard_map/all_to_all | solution.py:24
  156.0 4.1 %copy.48 = bf16[4,4,128,704]{2,1,0,3:T(4,128)(2,1)S(1)} copy(bf16[4,4,128,704]{2,3,0,1:T(8,128)(2,1)} %bitcast.55) | data formatting | bytes 5767168 | tf_op jit(solution)/shard_map/transpose | solution.py:80
  160.0 3.4 %reshape_reshape.18 = bf16[2048,704]{0,1:T(8,128)(2,1)} reshape(bf16[4,4,128,704]{2,1,0,3:T(4,128)(2,1)S(1)} %copy.48) | data formatting | bytes 5767168 | tf_op jit(solution)/shard_map/reshape;reshape | solution.py:32
  163.4 17.8 %all-to-all-done.5 = bf16[4,128,2048]{2,1,0:T(8,128)(2,1)} async-done(((bf16[4,128,2048]{2,1,0:T(8,128)(2,1)}), bf16[4,128,2048]{2,1,0:T(8,128)(2,1)}, u32[]{:S(2)}, u32[]{:S(2)}) %all-to-all-start.5) | async-done | bytes 2097184 | tf_op jit(solution)/shard_map/all_to_all | solution.py:24
  181.1 2.1 broadcast_in_dim.28
  183.3 8.9 %all_to_all.48 = bf16[2,4,128,2048]{3,2,1,0:T(8,128)(2,1)S(1)} all-to-all(bf16[2,4,128,2048]{3,2,1,0:T(8,128)(2,1)S(1)} %broadcast_in_dim.28), channel_id=1, replica_groups=mesh['rep'=2,'fs_0'=4,'fs_1'=4,'tp_0'=4,'tp_1'=2] {'tp_1'}, dimensions={0} | all-to-all | bytes 8388608 | tf_op jit(solution)/shard_map/all_to_all | solution.py:24
  192.2 2.3 copy.46
  194.5 7.9 %fusion.2 = f32[1024,704]{0,1:T(8,128)} fusion(bf16[1024,2048]{1,0:T(8,128)(2,1)} %bitcast.51, bf16[2048,1408]{0,1:T(8,128)(2,1)} %all-gather.5.cloned.1.call-done), kind=kOutput, calls=%fused_computation.8 | convolution fusion | flops 2952790016 | bytes 9961472 | tf_op jit(solution)/shard_map/dot_general | solution.py:158
  202.4 11.2 %convolution_convert_fusion = bf16[1024,2048]{1,0:T(8,128)(2,1)} fusion(bf16[2048,704]{0,1:T(8,128)(2,1)S(1)} %copy-done.1, f32[1024,704]{0,1:T(8,128)} %fusion.2, bf16[1024,2048]{1,0:T(8,128)(2,1)} %bitcast.52, bf16[2048,1408]{0,1:T(8,128)(2,1)} %all-gather.5.cloned.1.call-done), kind=kOutput, calls=%fused_computation.4 | convolution fusion | flops 5912002560 | bytes 17039360 | tf_op jit(solution)/shard_map/dot_general | solution.py:95
  213.7 2.5 copy.65
  216.2 8.1 %all_to_all.49 = bf16[2,4,128,2048]{3,2,1,0:T(8,128)(2,1)} all-to-all(bf16[2,4,128,2048]{3,2,1,0:T(8,128)(2,1)S(1)} %bitcast.50), channel_id=1, replica_groups=mesh['rep'=2,'fs_0'=4,'fs_1'=4,'tp_0'=4,'tp_1'=2] {'tp_1'}, dimensions={0} | all-to-all | bytes 8388608 | tf_op jit(solution)/shard_map/all_to_all | solution.py:62
  224.3 3.5 %reduce_sum.94 = bf16[4,128,2048]{2,1,0:T(8,128)(2,1)S(1)} reduce(bf16[2,4,128,2048]{3,2,1,0:T(8,128)(2,1)} %all_to_all.49, bf16[]{:T(256)} %constant.64.clone.1), dimensions={0}, to_apply=%region_7.8 | reduce | flops 1048576 | bytes 6291458 | tf_op jit(solution)/shard_map/reduce_sum | solution.py:63
  227.8 28.5 %all_to_all.50 = bf16[4,128,2048]{2,1,0:T(8,128)(2,1)S(1)} all-to-all(bf16[4,128,2048]{2,1,0:T(8,128)(2,1)S(1)} %reduce_sum.94), channel_id=1, replica_groups=mesh['rep'=2,'fs_0'=4,'fs_1'=4,'tp_0'=4,'tp_1'=2] {'tp_0'}, dimensions={0} | all-to-all | bytes 4194304 | tf_op jit(solution)/shard_map/all_to_all | solution.py:70
  (54 shorter events, 14.1 us)
Async XLA Ops:
  6.5 21.5 %copy-start = (bf16[128,2048]{1,0:T(8,128)(2,1)S(1)}, bf16[128,2048]{1,0:T(8,128)(2,1)}, u32[]{:S(2)}) copy-start(bf16[128,2048]{1,0:T(8,128)(2,1)} %param.13) | copy-start | bytes 1572868
  6.5 149.4 %all-gather.7.cloned.1.call-start = ((), (), s32[]{:S(2)}) async-start(), calls=%async_computation.10 | async-start | bytes 3604480 | tf_op jit(solution)/shard_map/all_gather | solution.py:77
  25.5 169.0 %all-gather.5.cloned.1.call-start = ((), (), s32[]{:S(2)}) async-start(), calls=%async_computation.9 | async-start | bytes 6127616 | tf_op jit(solution)/shard_map/all_gather | solution.py:18
  28.0 6.2 %copy-start.6 = (bf16[512]{0:T(512)(128)(2,1)S(1)}, bf16[512]{0:T(512)(128)(2,1)}, u32[]{:S(2)}) copy-start(bf16[512]{0:T(512)(128)(2,1)} %param.18) | copy-start | bytes 3076
  28.0 6.2 %copy-start.7 = (bf16[512]{0:T(512)(128)(2,1)S(1)}, bf16[512]{0:T(512)(128)(2,1)}, u32[]{:S(2)}) copy-start(bf16[512]{0:T(512)(128)(2,1)} %param.17) | copy-start | bytes 3076
  28.0 6.3 %copy-start.2 = (bf16[128,64]{0,1:T(8,128)(2,1)S(1)}, bf16[128,64]{0,1:T(8,128)(2,1)}, u32[]{:S(2)}) copy-start(bf16[128,64]{0,1:T(8,128)(2,1)} %param.21) | copy-start | bytes 49156
  28.0 6.3 %copy-start.3 = (bf16[128,64]{0,1:T(8,128)(2,1)S(1)}, bf16[128,64]{0,1:T(8,128)(2,1)}, u32[]{:S(2)}) copy-start(bf16[128,64]{0,1:T(8,128)(2,1)} %param.16) | copy-start | bytes 49156
  28.0 6.3 %copy-start.4 = (bf16[128,64]{0,1:T(8,128)(2,1)S(1)}, bf16[128,64]{0,1:T(8,128)(2,1)}, u32[]{:S(2)}) copy-start(bf16[128,64]{0,1:T(8,128)(2,1)} %param.15) | copy-start | bytes 49156
  30.0 43.6 %all-to-all-start = ((bf16[4,128,2048]{2,1,0:T(8,128)(2,1)}), bf16[4,128,2048]{2,1,0:T(8,128)(2,1)S(1)}, u32[]{:S(2)}, u32[]{:S(2)}) async-start(bf16[4,128,2048]{2,1,0:T(8,128)(2,1)} %broadcast_in_dim.22), calls=%async_computation | async-start | bytes 4194304 | tf_op jit(solution)/shard_map/all_to_all | solution.py:24
  90.2 7.7 %copy-start.8 = (bf16[4,128]{1,0:T(4,128)(2,1)S(1)}, bf16[4,128]{1,0:T(4,128)(2,1)}, u32[]{:S(2)}) copy-start(bf16[4,128]{1,0:T(4,128)(2,1)} %param.20) | copy-start | bytes 3076
  92.5 10.6 %all-to-all-start.2 = ((f32[8,1,2048]{2,1,0:T(1,128)}), f32[8,1,2048]{2,1,0:T(1,128)S(1)}, u32[]{:S(2)}, u32[]{:S(2)}) async-start(f32[8,1,2048]{2,1,0:T(1,128)} %broadcast_in_dim.24), calls=%async_computation.2 | async-start | bytes 131072 | tf_op jit(solution)/shard_map/all_to_all | solution.py:24
  114.2 8.7 %copy-start.5 = (bf16[2048]{0:T(1024)(128)(2,1)S(1)}, bf16[2048]{0:T(1024)(128)(2,1)}, u32[]{:S(2)}) copy-start(bf16[2048]{0:T(1024)(128)(2,1)} %param.22) | copy-start | bytes 12292
  119.4 29.6 %all-to-all-start.4 = ((bf16[4,128,2048]{2,1,0:T(8,128)(2,1)}), bf16[4,128,2048]{2,1,0:T(8,128)(2,1)S(1)}, u32[]{:S(2)}, u32[]{:S(2)}) async-start(bf16[4,128,2048]{2,1,0:T(8,128)(2,1)} %reduce_sum.91), calls=%async_computation.4 | async-start | bytes 4194304 | tf_op jit(solution)/shard_map/all_to_all | solution.py:70
  151.5 29.7 %all-to-all-start.5 = ((bf16[4,128,2048]{2,1,0:T(8,128)(2,1)}), bf16[4,128,2048]{2,1,0:T(8,128)(2,1)}, u32[]{:S(2)}, u32[]{:S(2)}) async-start(bf16[4,128,2048]{2,1,0:T(8,128)(2,1)} %broadcast_in_dim.27), calls=%async_computation.5 | async-start | bytes 4194304 | tf_op jit(solution)/shard_map/all_to_all | solution.py:24
  194.5 7.9 %copy-start.1 = (bf16[2048,704]{0,1:T(8,128)(2,1)S(1)}, bf16[2048,704]{0,1:T(8,128)(2,1)}, u32[]{:S(2)}) copy-start(bf16[2048,704]{0,1:T(8,128)(2,1)} %reshape_reshape.18) | copy-start | bytes 8650756
Sparse Core Ops, SparseCore 0:
  25.6 49.8 all-gather.6
  77.2 92.0 all-gather.4
where the time goes:
time: 265 us
  blocking collectives  126 us (48%)
  waiting for transfers between devices  49 us (18%)
  matrix products  23 us (9%)
  local copies, waits for them, and re-layouts  20.9 us (8%)
  starting transfers between devices  17.7 us (7%)
  other arithmetic  14 us (5%)
  between operations  13.6 us (5%)
    all_gather x1, blocking collectives, side_by_side(): out = lax.all_gather(both, axis, axis=dim, tiled=True)  39.3 us
    all_to_all x1, blocking collectives, summed_rows(): lax.all_to_all(own.astype(jnp.bfloat16), far, 0, 0, tiled=True)  28.5 us
    all_to_all x1, waiting for transfers between devices, summed_rows(): lax.all_to_all(own.astype(jnp.bfloat16), far, 0, 0, tiled=True)  26 us
    all_to_all x2, blocking collectives, sent_to_all(): lax.all_to_all(jnp.broadcast_to(value[None], (count, *value.shape)), axis...  24.4 us
    all_to_all x3, waiting for transfers between devices, sent_to_all(): lax.all_to_all(jnp.broadcast_to(value[None], (count, *value.shape)), axis...  23 us
    all_gather x1, blocking collectives, gather_in_order(): blocks = lax.all_gather(blocks, axes[k])  17.9 us
    all_to_all x2, blocking collectives, summed_on_arrival(): blocks = lax.all_to_all(split_up(value, dim, count), axis, 0, 0, tiled=True)  16.3 us
    all_to_all x3, starting transfers between devices, sent_to_all(): lax.all_to_all(jnp.broadcast_to(value[None], (count, *value.shape)), axis...  14 us
  transfers between devices with their start and end apart: 6, of which 3 were waited for; matrix products, arithmetic and copies ran while one was open for 11% of the time, Pallas kernels for 0%

commit v1 on v0

v1 whole, which is shorter than its diff:
```python
import functools

import jax
import jax.numpy as jnp
from jax import lax
from jax.experimental import pallas as pl
from jax.experimental.pallas import tpu as pltpu
from jax.sharding import Mesh
from jax.sharding import PartitionSpec as P

AXES = ("rep", "fs_0", "fs_1", "tp_0", "tp_1")
FS = ("fs_0", "fs_1")
TP = ("tp_0", "tp_1")
EPS = 1e-06
N = 4
COPIES = 192
BF, F32 = jnp.bfloat16, jnp.float32


def dot_nt(left, right):
    return lax.dot_general(left, right, (((1,), (1,)), ((), ())), preferred_element_type=F32)


def gelu(v):
    return v * (0.5 * (1.0 + jnp.tanh(0.7978845608028654 * (v + 0.044715 * (v * v * v)))))


def cat(parts, axis):
    return jnp.concatenate(parts, axis=axis) if len(parts) > 1 else parts[0]


def kernel(
    tokens, gate_proj, value_proj, out_proj, ffn_gate, ffn_up, ffn_down, params, mix_kernel,
    out,
    tok, par, mixk, vw, gw, ow, a_gu, b_gu, a_d, b_d, nbuf, middle, xall, hidden, parts, r1, r2,
    lsem, ssem, rsem,
):
    rep = lax.axis_index("rep")
    zi, xi, yi, ci = (lax.axis_index(a) for a in AXES[1:])

    def wrap(i, s):
        return lax.rem(i + (s + N), N)

    def device(axis, s):
        if axis == "z":
            z = lax.rem(rep * N + zi + (s + 2 * N), 2 * N)
            return {"rep": z // N, "fs_0": lax.rem(z, N)}
        if axis == "c":
            return {"tp_1": 1 - ci}
        name, i = {"x": ("fs_1", xi), "y": ("tp_0", yi)}[axis]
        return {name: wrap(i, s)}

    index = {"x": xi, "y": yi, "z": zi}
    sends = []

    def push(axis, s, mine, theirs):
        k = len(sends)
        to = device(axis, s)
        copy = pltpu.make_async_remote_copy(
            mine, mine, ssem.at[k], rsem.at[k], device_id=to, device_id_type=pl.DeviceIdType.MESH
        )
        copy.start()
        sends.append(copy)
        arrival = pltpu.make_async_remote_copy(
            theirs, theirs, ssem.at[k], rsem.at[k], device_id=to,
            device_id_type=pl.DeviceIdType.MESH,
        )
        return arrival.wait_recv

    locals_ = []

    def load(src, dst):
        copy = pltpu.make_async_copy(src, dst, lsem.at[len(locals_)])
        copy.start()
        locals_.append(copy)
        return copy.wait

    half = a_d.shape[-2]
    own_v = load(value_proj, vw.at[ci, yi, xi, zi])
    own_g = load(gate_proj, gw.at[ci, xi, zi, yi])
    own_o = load(out_proj, ow.at[ci, zi, yi, xi])
    own_gu = [
        load(ffn_gate.at[pl.ds(0, half)], a_gu.at[ci, xi, zi, 0]),
        load(ffn_up.at[pl.ds(0, half)], a_gu.at[ci, xi, zi, 1]),
        load(ffn_gate.at[pl.ds(half, half)], b_gu.at[ci, zi, xi, 0]),
        load(ffn_up.at[pl.ds(half, half)], b_gu.at[ci, zi, xi, 1]),
    ]
    got_tok = load(tokens, tok)
    got_par = load(params, par)
    own_d = [
        load(ffn_down.at[pl.ds(0, half)], a_d.at[ci, xi, zi]),
        load(ffn_down.at[pl.ds(half, half)], b_d.at[ci, zi, xi]),
    ]
    got_mixk = load(mix_kernel, mixk)

    barrier = pltpu.get_barrier_semaphore()
    greeted = [(a, s) for a in "xyz" for s in (1, -1, 2)] + [("z", -2), ("c", 1)]
    for a, s in greeted:
        pl.semaphore_signal(
            barrier, inc=1, device_id=device(a, s), device_id_type=pl.DeviceIdType.MESH
        )
    pl.semaphore_wait(barrier, len(greeted))

    def direct(axis, group, halves):
        i = index[axis]
        got = [
            push(axis, 1, group(i), group(wrap(i, -1))),
            push(axis, -1, group(i), group(wrap(i, 1))),
        ]
        far = wrap(i, 2)
        if axis == "z":
            got += [push(axis, 2, halves(i, 0), halves(far, 0)),
                    push(axis, -2, halves(i, 1), halves(far, 1))]
        else:
            got += [push(axis, 2, group(i), group(far))]
        return got

    class Ring:
        def __init__(self, axis, halves):
            self.axis, self.halves, self.i = axis, halves, index[axis]
            i = self.i
            before, after = wrap(i, -1), wrap(i, 1)
            self.first = [push(axis, 1, halves(i, 0), halves(before, 0)),
                          push(axis, -1, halves(i, 1), halves(after, 1))]
            self.second = [push(axis, 1, halves(i, 1), halves(before, 1)),
                           push(axis, -1, halves(i, 0), halves(after, 0))]

        def relay(self):
            i, h = self.i, self.halves
            before, after, far = wrap(i, -1), wrap(i, 1), wrap(i, 2)
            self.first[0]()
            up = push(self.axis, 1, h(before, 0), h(far, 0))
            self.first[1]()
            down = push(self.axis, -1, h(after, 1), h(far, 1))
            self.last = [up, down]

        def near(self):
            for w in self.second:
                w()

        def end(self):
            for w in self.last:
                w()

    def pair(n):
        return lambda h: pl.ds(h * (n // 2), n // 2)

    rows = pair(vw.shape[-2])
    two = pair(N)
    own_v()
    v1 = direct("z", lambda i: vw.at[ci, yi, xi, i], lambda i, h: vw.at[ci, yi, xi, i, rows(h)])
    own_g()
    g1 = direct("y", lambda i: gw.at[ci, xi, zi, i], None)
    own_o()
    o1 = direct("x", lambda i: ow.at[ci, zi, yi, i], None)
    for w in v1:
        w()
    v2 = direct("x", lambda i: vw.at[ci, yi, i], None)
    for w in g1:
        w()
    g2 = direct("z", lambda i: gw.at[ci, xi, i], lambda i, h: gw.at[ci, xi, i, two(h)])
    for w in o1:
        w()
    o2 = direct("y", lambda i: ow.at[ci, zi, i], None)

    for w in own_gu:
        w()
    agu1 = Ring("z", lambda i, h: a_gu.at[ci, xi, i, h])
    bgu1 = Ring("x", lambda i, h: b_gu.at[ci, zi, i, h])

    fwd_v, fwd_g, fwd_o = [], [], []

    def forward(keep, ref_of):
        keep.append(push("c", 1, ref_of(ci), ref_of(1 - ci)))

    for w in v2:
        w()
    v3 = Ring("y", lambda i, h: vw.at[ci, i, two(h)])
    forward(fwd_v, lambda c: vw.at[c, yi])
    for w in g2:
        w()
    g3 = Ring("x", lambda i, h: gw.at[ci, i, two(h)])
    forward(fwd_g, lambda c: gw.at[c, xi])
    for w in o2:
        w()
    o3 = Ring("z", lambda i, h: ow.at[ci, i, two(h)])
    forward(fwd_o, lambda c: ow.at[c, zi])

    agu1.relay()
    bgu1.relay()
    v3.relay()
    g3.relay()
    o3.relay()
    agu1.near()
    bgu1.near()
    agu1.end()
    bgu1.end()
    agu2 = Ring("x", lambda i, h: a_gu.at[ci, i, two(h)])
    bgu2 = Ring("z", lambda i, h: b_gu.at[ci, i, two(h)])
    fwd_gu = []
    forward(fwd_gu, lambda c: a_gu.at[c, xi])
    forward(fwd_gu, lambda c: b_gu.at[c, zi])
    for w in own_d:
        w()
    ad1 = Ring("z", lambda i, h: a_d.at[ci, xi, i, pl.ds(h * (half // 2), half // 2)])
    bd1 = Ring("x", lambda i, h: b_d.at[ci, zi, i, pl.ds(h * (half // 2), half // 2)])

    def finish(ring, keep, ref, i):
        ring.near()
        forward(keep, lambda c: ref.at[c, wrap(i, -1)])
        forward(keep, lambda c: ref.at[c, wrap(i, 1)])
        ring.end()
        forward(keep, lambda c: ref.at[c, wrap(i, 2)])

    got_tok()
    got_par()
    got_mixk()
    floats = tok[...].astype(F32)
    scale = lax.rsqrt(jnp.mean(floats * floats, axis=-1, keepdims=True) + EPS)
    nbuf[...] = (floats * scale * par[0:1, :]).astype(BF)

    finish(v3, fwd_v, vw, yi)
    finish(g3, fwd_g, gw, xi)
    finish(o3, fwd_o, ow, zi)
    for w in fwd_v:
        w()

    every = [(z, x) for z in range(N) for x in range(N)]

    def project(block, lo):
        cols = [
            cat([block(c, y, z, x) for y in (lo, lo + 1) for c in range(2)], 0) for z, x in every
        ]
        return dot_nt(nbuf[...], cat(cols, 1))

    width = 512
    activated = gelu(cat([project(lambda c, y, z, x: vw[c, y, x, z], lo) for lo in (0, 2)], 1))
    center = jnp.sum(activated, axis=-1, keepdims=True) / width
    spread = jnp.sum(activated * activated, axis=-1, keepdims=True) / width - center * center
    values = (
        (activated - center) * lax.rsqrt(spread + EPS) * par[2:3, 0:width]
        + par[2:3, width : 2 * width]
    ).astype(BF)
    span, groups = mixk.shape[1], mixk.shape[0]
    t_pos = lax.broadcasted_iota(jnp.int32, (span, span), 0)
    s_pos = lax.broadcasted_iota(jnp.int32, (span, span), 1)
    mixing = []
    for g in range(groups):
        masked = jnp.where(s_pos <= t_pos, mixk[g].astype(F32), 0.0).astype(BF)
        offset_row = par[2:3, 2 * width + g * span : 2 * width + (g + 1) * span]
        offset = jnp.sum(jnp.where(s_pos == t_pos, offset_row, 0.0), axis=-1, keepdims=True)
        mixing.append(
            jnp.dot(masked, values[:, g * span : (g + 1) * span], preferred_element_type=F32)
            + offset
        )
    for w in fwd_g:
        w()
    gate_u = gelu(cat([project(lambda c, y, z, x: gw[c, x, z, y], lo) for lo in (0, 2)], 1))
    gated = (gate_u * cat(mixing, 1)).astype(BF)
    for w in fwd_o:
        w()
    total = jnp.zeros((span, 1), F32)
    lane = 128
    for z in range(N):
        weights = cat(
            [
                cat([ow[c, z, y, x] for y in range(N) for c in range(2)], 0)
                for x in range(N)
            ],
            1,
        )
        cols = slice(z * N * lane, (z + 1) * N * lane)
        mid = (
            tok[:, cols].astype(F32) + jnp.dot(gated, weights, preferred_element_type=F32)
        ).astype(BF)
        middle[:, cols] = mid
        mid = mid.astype(F32)
        total += jnp.sum(mid * mid, axis=-1, keepdims=True)
    width2 = middle.shape[1]
    scale2 = lax.rsqrt(total / width2 + EPS)
    xall[yi] = (middle[...].astype(F32) * scale2 * par[1:2, :]).astype(BF)

    toks = Ring("y", lambda i, h: xall.at[i, pl.ds(h * (span // 2), span // 2)])

    ad1.relay()
    bd1.relay()
    agu2.relay()
    bgu2.relay()
    ad1.near()
    bd1.near()
    ad1.end()
    bd1.end()

    order = [zi, wrap(zi, -1), wrap(zi, 1), wrap(zi, 2)]
    before, after, far = wrap(xi, -1), wrap(xi, 1), wrap(xi, 2)
    hr = half // 2
    bd2 = Ring("z", lambda i, h: b_d.at[ci, i, two(h)])
    ad2 = []
    for z in order:
        ad2.append([push("x", 1, a_d.at[ci, xi, z], a_d.at[ci, before, z]),
                    push("x", -1, a_d.at[ci, xi, z], a_d.at[ci, after, z])])
    ad2_last = []

    def down_relay(k):
        z = order[k]
        ad2[k][0]()
        up = push("x", 1, a_d.at[ci, before, z, pl.ds(0, hr)], a_d.at[ci, far, z, pl.ds(0, hr)])
        ad2[k][1]()
        down = push(
            "x", -1, a_d.at[ci, after, z, pl.ds(hr, hr)], a_d.at[ci, far, z, pl.ds(hr, hr)]
        )
        ad2_last.append([up, down])

    toks.relay()
    finish(agu2, fwd_gu, a_gu, xi)
    finish(bgu2, fwd_gu, b_gu, zi)
    toks.near()
    toks.end()
    for w in fwd_gu:
        w()

    full = 4 * half

    def unit_rows(which, lo, hi):
        pieces = []
        for seg in range(4):
            a, b = max(lo, seg * half), min(hi, (seg + 1) * half)
            if a < b:
                c, h = divmod(seg, 2)
                r = slice(a - seg * half, b - seg * half)
                ref = (a_gu, b_gu)[h]
                pieces.append(
                    cat(
                        [
                            ref[(c, x, z) + (which, r)] if h == 0 else ref[(c, z, x) + (which, r)]
                            for z, x in every
                        ],
                        1,
                    )
                )
        return cat(pieces, 0)

    rows_all = xall.reshape(N * span, width2)
    step = 256
    relayed = 0
    for lo in range(0, full, step):
        hi = min(lo + step, full)
        if hi - lo == step:
            gate_pre = dot_nt(rows_all[...], unit_rows(0, lo, hi))
            up_pre = dot_nt(rows_all[...], unit_rows(1, lo, hi))
        else:
            both = dot_nt(
                rows_all[...], cat([unit_rows(0, lo, hi), unit_rows(1, lo, hi)], 0)
            )
            gate_pre, up_pre = both[:, : hi - lo], both[:, hi - lo :]
        hidden[:, lo:hi] = (gate_pre * lax.logistic(gate_pre) * up_pre).astype(BF)
        if lo == 2 * step:
            bd2.relay()
        if lo == 4 * step:
            down_relay(0)

    got_r1, got_r2, ahead, back = {}, {}, wrap(yi, 1), wrap(yi, -1)
    opposite = wrap(yi, 2)

    def sum_first(k):
        z = order[k]
        got_r1[k] = [
            send_to("y", 1, parts.at[opposite, z, two(0)], r1.at[0, k]),
            send_to("y", -1, parts.at[opposite, z, two(1)], r1.at[1, k]),
        ]
        got_r2[k] = [
            send_to("y", 1, parts.at[ahead, z, two(1)], r2.at[0, k, two(1)]),
            send_to("y", -1, parts.at[back, z, two(0)], r2.at[1, k, two(0)]),
        ]

    def send_to(axis, s, src, dst):
        k = len(sends)
        copy = pltpu.make_async_remote_copy(
            src, dst, ssem.at[k], rsem.at[k], device_id=device(axis, s),
            device_id_type=pl.DeviceIdType.MESH,
        )
        copy.start()
        sends.append(copy)
        return copy.wait_recv

    def sum_second(k):
        z = order[k]
        got_r1[k][0]()
        parts[ahead, z, two(0)] = (
            parts[ahead, z, two(0)].astype(F32) + r1[0, k].astype(F32)
        ).astype(BF)
        got_r2[k].append(send_to("y", 1, parts.at[ahead, z, two(0)], r2.at[0, k, two(0)]))
        got_r1[k][1]()
        parts[back, z, two(1)] = (
            parts[back, z, two(1)].astype(F32) + r1[1, k].astype(F32)
        ).astype(BF)
        got_r2[k].append(send_to("y", -1, parts.at[back, z, two(1)], r2.at[1, k, two(1)]))

    def sum_last(k):
        z = order[k]
        for w in got_r2[k]:
            w()
        for x in range(N):
            summed = (
                parts[yi, z, x].astype(F32) + r2[0, k, x].astype(F32) + r2[1, k, x].astype(F32)
            )
            cols = pl.ds(pl.multiple_of((z * N + x) * lane, lane), lane)
            out[:, cols] = (middle[:, cols].astype(F32) + summed).astype(BF)

    def chunk(k):
        z = order[k]
        if k == 1:
            bd2.near()
        if k == 3:
            bd2.end()
        for w in ad2_last[k]:
            w()
        fwd = []
        forward(fwd, lambda c: a_d.at[c, :, z])
        forward(fwd, lambda c: b_d.at[c, z])
        if k + 1 < N:
            down_relay(k + 1)
        for w in fwd:
            w()
        for x2 in range(0, N, 2):
            weights = cat(
                [
                    cat([ref for c in range(2) for ref in (a_d[c, x, z], b_d[c, z, x])], 0)
                    for x in (x2, x2 + 1)
                ],
                1,
            )
            result = jnp.dot(hidden[...], weights, preferred_element_type=F32).astype(BF)
            for y in range(N):
                for j in range(2):
                    parts[y, z, x2 + j] = result[
                        y * span : (y + 1) * span, j * lane : (j + 1) * lane
                    ]

    for k in range(N):
        chunk(k)
        sum_first(k)
        if k:
            sum_second(k - 1)
        if k > 1:
            sum_last(k - 2)
    sum_second(N - 1)
    sum_last(N - 2)
    sum_last(N - 1)
    for copy in sends:
        copy.wait_send()


def per_device(
    tokens, mix_gain, gate_proj, value_proj, layer_gain, layer_shift, mix_kernel, mix_offset,
    out_proj, ffn_gain, ffn_gate, ffn_up, ffn_down,
):
    span, width = tokens.shape
    units, lane = ffn_gate.shape[1], ffn_gate.shape[0]
    channels = layer_gain.shape[0]
    local = gate_proj.shape[1]
    half = units // 2
    small = jnp.concatenate(
        [layer_gain, layer_shift, mix_offset.reshape(-1)]
        + [jnp.zeros((width - 3 * channels,), BF)]
    )
    params = jnp.stack([mix_gain, ffn_gain, small] + [jnp.zeros_like(mix_gain)] * 5).astype(F32)
    anywhere = pl.BlockSpec(memory_space=pl.ANY)
    return pl.pallas_call(
        kernel,
        out_shape=jax.ShapeDtypeStruct(tokens.shape, BF),
        in_specs=[anywhere] * 9,
        out_specs=pl.BlockSpec(memory_space=pltpu.VMEM),
        scratch_shapes=[
            pltpu.VMEM((span, width), BF),
            pltpu.VMEM(params.shape, F32),
            pltpu.VMEM(mix_kernel.shape, BF),
            pltpu.VMEM((2, N, N, N, local, lane), BF),
            pltpu.VMEM((2, N, N, N, local, lane), BF),
            pltpu.VMEM((2, N, N, N, local, lane), BF),
            pltpu.VMEM((2, N, N, 2, half, lane), BF),
            pltpu.VMEM((2, N, N, 2, half, lane), BF),
            pltpu.VMEM((2, N, N, half, lane), BF),
            pltpu.VMEM((2, N, N, half, lane), BF),
            pltpu.VMEM((span, width), BF),
            pltpu.VMEM((span, width), BF),
            pltpu.VMEM((N, span, width), BF),
            pltpu.VMEM((N * span, 2 * units), BF),
            pltpu.VMEM((N, N, N, span, lane), BF),
            pltpu.VMEM((2, N, N // 2, span, lane), BF),
            pltpu.VMEM((2, N, N, span, lane), BF),
            pltpu.SemaphoreType.DMA((16,)),
            pltpu.SemaphoreType.DMA((COPIES,)),
            pltpu.SemaphoreType.DMA((COPIES,)),
        ],
        compiler_params=pltpu.CompilerParams(
            collective_id=0, has_side_effects=True, vmem_limit_bytes=63 * 2**20
        ),
    )(
        tokens, gate_proj.T, value_proj.T, out_proj.T, ffn_gate.T, ffn_up.T, ffn_down.T, params,
        mix_kernel,
    )


def solution(mesh):
    torus = Mesh(mesh.devices.reshape(mesh.shape["rep"], 4, 4, 4, 2), AXES)
    return jax.shard_map(
        per_device,
        mesh=torus,
        in_specs=(
            P(AXES, None), P(), P(FS, TP), P(FS, TP), P(), P(), P(), P(), P(FS, TP), P(),
            P(FS, TP), P(FS, TP), P(FS, TP),
        ),
        out_specs=P(AXES, None),
        check_vma=False,
    )
```

time: 265 us -> 107 us (0.40)
  blocking collectives: 126 us -> 0 us
  Pallas kernels: 0 us -> 102 us
  waiting for transfers between devices: 49 us -> 0 us
  matrix products: 23 us -> 0 us
  starting transfers between devices: 17.7 us -> 0 us
  local copies, waits for them, and re-layouts: 20.9 us -> 4.03 us
  between operations: 13.6 us -> 0.05 us
  other arithmetic: 14 us -> 0.65 us
    pallas_call x0 -> x1, Pallas kernels: none -> 102 us  [per_device(): pl.pallas_call(kernel, out_shape=jax.ShapeDtypeStruct(tokens.shape, BF),...]
    all_to_all x5 -> x0, blocking collectives: 69.1 us -> none  [the longest x1 28.5 us: summed_rows(): lax.all_to_all(own.astype(jnp.bfloat16), far, 0, 0, tiled=True)]
    all_gather x2 -> x0, blocking collectives: 57.2 us -> none  [the longest x1 39.3 us: side_by_side(): out = lax.all_gather(both, axis, axis=dim, tiled=True)]
    all_to_all x4 -> x0, waiting for transfers between devices: 49 us -> none  [the longest x1 26 us: summed_rows(): lax.all_to_all(own.astype(jnp.bfloat16), far, 0, 0, tiled=True)]
    dot_general x5 -> x0, matrix products: 23 us -> none  [the longest x2 12.5 us: contract_last(): lax.dot_general(left, right, (((1,), (1,)), ((), ())), preferred_element_...]
    all_to_all x4 -> x0, starting transfers between devices: 17.6 us -> none  [the longest x3 14 us: sent_to_all(): lax.all_to_all(jnp.broadcast_to(value[None], (count, *value.shape)), axis...]
    reduce_sum x8 -> x0, other arithmetic: 10 us -> none  [the longest x2 8.66 us: summed_on_arrival(): return jnp.sum(blocks.astype(jnp.float32), axis=0)]
    broadcast_in_dim x5 -> x1, local copies, waits for them, and re-layouts: 6.5 us -> 0.01 us  [per_device(): jnp.zeros((width - 3 * channels,), BF)]
  transfers between devices with their start and end apart: 6 -> 0, of which waited for: 3 -> 0; matrix products, arithmetic and copies ran while one was open for 11% -> 0% of each run, Pallas kernels for 0% -> 0%
where the time goes in v1:
time: 107 us
  Pallas kernels  102 us (95%)
  local copies, waits for them, and re-layouts  4.03 us (4%)
    pallas_call x1, Pallas kernels, per_device(): pl.pallas_call(kernel, out_shape=jax.ShapeDtypeStruct(tokens.shape, BF),...  102 us
    unnamed x11, local copies, waits for them, and re-layouts  3.92 us

profile of v1, /device:TPU:1, one launch (start us, length us, event | category | flops | bytes accessed | tf_op | source)
XLA Modules:
  0.0 107.1 jit_solution(14524330566960165105)
XLA Ops:
  0.0 0.0 copy-start.3
  0.0 0.0 copy-start.4
  0.0 0.0 copy-start.2
  0.0 0.7 copy-done.3
  0.7 0.0 copy-done.4
  0.7 0.0 copy-done.2
  0.7 0.0 copy-start
  0.7 0.7 copy-done
  1.4 0.0 copy-start.1
  1.4 0.7 copy-done.1
  2.1 0.1 stack.19
  2.2 0.6 convert_element_type.3.params
  2.8 102.4 %shard_map.127 = bf16[128,2048]{1,0:T(8,128)(2,1)} custom-call(bf16[128,2048]{1,0:T(8,128)(2,1)} %tokens.1, bf16[64,128]{1,0:T(8,128)(2,1)} %bitcast.10, bf16[64,128]{1,0:T(8,128)(2,1)} %bitcast.11, bf16[64,128]{1,0:T(8,128)(2,1)} %bitcast.12, bf16[704,128]{1,0:T(8,128)(2,1)} %bitcast.7, bf16[704,128]{1,0:T(8,128)(2,1)} %bitcast.8, ...), custom_call_target="tpu_custom_call" | custom-call | tf_op jit(solution)/shard_map/pallas_call | solution.py:469
  105.2 1.9 %copy.15 = bf16[128,2048]{1,0:T(8,128)(2,1)} copy(bf16[128,2048]{1,0:T(8,128)(2,1)} %shard_map.127) | data formatting | bytes 1048576
  (7 shorter events, 0.0 us)
Async XLA Ops:
  0.0 0.7 copy-start.3
  0.0 0.7 copy-start.4
  0.0 0.7 copy-start.2
  0.7 0.7 copy-start
  1.4 0.7 copy-start.1

commit v2 on v1

v2 whole, which is shorter than its diff:
```python
import functools

import jax
import jax.numpy as jnp
from jax import lax
from jax.experimental import pallas as pl
from jax.experimental.pallas import tpu as pltpu
from jax.sharding import Mesh
from jax.sharding import PartitionSpec as P

AXES = ("rep", "fs_0", "fs_1", "tp_0", "tp_1")
FS = ("fs_0", "fs_1")
TP = ("tp_0", "tp_1")
EPS = 1e-06
N = 4
COPIES = 216


def row_waves(half):
    return [(0, 128), (128, 128), (256, half - 256)]

BF, F32 = jnp.bfloat16, jnp.float32


def dot_nt(left, right):
    return lax.dot_general(left, right, (((1,), (1,)), ((), ())), preferred_element_type=F32)


def gelu(v):
    return v * (0.5 * (1.0 + jnp.tanh(0.7978845608028654 * (v + 0.044715 * (v * v * v)))))


def row(ref):
    return ref[...].astype(F32).reshape(1, -1)


def cat(parts, axis):
    return jnp.concatenate(parts, axis=axis) if len(parts) > 1 else parts[0]


def kernel(
    tokens, gate_proj, value_proj, out_proj, ffn_gate, ffn_up, ffn_down, mix_gain, layer_gain,
    layer_shift, mix_kernel, mix_offset, ffn_gain,
    out,
    tok, gain1, gain2, lgain, lshift, mixo, mixk, vw, gw, ow, a_gu, b_gu, a_d, b_d, nbuf, middle, xall, hidden, parts, r1, r2,
    lsem, ssem, rsem,
):
    rep = lax.axis_index("rep")
    zi, xi, yi, ci = (lax.axis_index(a) for a in AXES[1:])

    def wrap(i, s):
        return lax.rem(i + (s + N), N)

    def device(axis, s):
        if axis == "z":
            z = lax.rem(rep * N + zi + (s + 2 * N), 2 * N)
            return {"rep": z // N, "fs_0": lax.rem(z, N)}
        if axis == "c":
            return {"tp_1": 1 - ci}
        name, i = {"x": ("fs_1", xi), "y": ("tp_0", yi)}[axis]
        return {name: wrap(i, s)}

    index = {"x": xi, "y": yi, "z": zi}
    sends = []

    def push(axis, s, mine, theirs):
        k = len(sends)
        to = device(axis, s)
        copy = pltpu.make_async_remote_copy(
            mine, mine, ssem.at[k], rsem.at[k], device_id=to, device_id_type=pl.DeviceIdType.MESH
        )
        copy.start()
        sends.append(copy)
        arrival = pltpu.make_async_remote_copy(
            theirs, theirs, ssem.at[k], rsem.at[k], device_id=to,
            device_id_type=pl.DeviceIdType.MESH,
        )
        return arrival.wait_recv

    locals_ = []

    def load(src, dst):
        copy = pltpu.make_async_copy(src, dst, lsem.at[len(locals_)])
        copy.start()
        locals_.append(copy)
        return copy.wait

    half = a_d.shape[-2]
    hr = half // 2
    waves = row_waves(half)
    half = a_d.shape[-2]
    hr = half // 2
    own_v = load(value_proj, vw.at[ci, yi, xi, zi])
    own_g = load(gate_proj, gw.at[ci, xi, zi, yi])
    own_o = load(out_proj, ow.at[ci, zi, yi, xi])
    own_gu = [
        load(src.at[pl.ds(h * half, half)], dst.at[j])
        for h, dst in ((0, a_gu.at[ci, xi, zi]), (1, b_gu.at[ci, zi, xi]))
        for j, src in ((0, ffn_gate), (1, ffn_up))
    ]
    got_tok = load(tokens, tok)
    own_d = [
        load(ffn_down.at[pl.ds(0, half)], a_d.at[ci, xi, zi]),
        load(ffn_down.at[pl.ds(half, half)], b_d.at[ci, zi, xi]),
    ]
    got_small = [
        load(src, dst)
        for src, dst in (
            (mix_gain, gain1), (layer_gain, lgain), (layer_shift, lshift), (mix_kernel, mixk),
            (mix_offset, mixo), (ffn_gain, gain2),
        )
    ]

    barrier = pltpu.get_barrier_semaphore()
    greeted = [(a, s) for a in "xyz" for s in (1, -1, 2)] + [("z", -2), ("c", 1)]
    for a, s in greeted:
        pl.semaphore_signal(
            barrier, inc=1, device_id=device(a, s), device_id_type=pl.DeviceIdType.MESH
        )
    pl.semaphore_wait(barrier, len(greeted))

    def direct(axis, group, halves):
        i = index[axis]
        got = [
            push(axis, 1, group(i), group(wrap(i, -1))),
            push(axis, -1, group(i), group(wrap(i, 1))),
        ]
        far = wrap(i, 2)
        if axis == "z":
            got += [push(axis, 2, halves(i, 0), halves(far, 0)),
                    push(axis, -2, halves(i, 1), halves(far, 1))]
        else:
            got += [push(axis, 2, group(i), group(far))]
        return got

    class Ring:
        def __init__(self, axis, halves):
            self.axis, self.halves, self.i = axis, halves, index[axis]
            i = self.i
            before, after = wrap(i, -1), wrap(i, 1)
            self.first = [push(axis, 1, halves(i, 0), halves(before, 0)),
                          push(axis, -1, halves(i, 1), halves(after, 1))]
            self.second = [push(axis, 1, halves(i, 1), halves(before, 1)),
                           push(axis, -1, halves(i, 0), halves(after, 0))]

        def relay(self):
            i, h = self.i, self.halves
            before, after, far = wrap(i, -1), wrap(i, 1), wrap(i, 2)
            self.first[0]()
            up = push(self.axis, 1, h(before, 0), h(far, 0))
            self.first[1]()
            down = push(self.axis, -1, h(after, 1), h(far, 1))
            self.last = [up, down]

        def near(self):
            for w in self.second:
                w()

        def end(self):
            for w in self.last:
                w()

    def pair(n):
        return lambda h: pl.ds(h * (n // 2), n // 2)

    rows = pair(vw.shape[-2])
    two = pair(N)
    own_v()
    v1 = direct("z", lambda i: vw.at[ci, yi, xi, i], lambda i, h: vw.at[ci, yi, xi, i, rows(h)])
    own_g()
    g1 = direct("y", lambda i: gw.at[ci, xi, zi, i], None)
    own_o()
    o1 = direct("x", lambda i: ow.at[ci, zi, yi, i], None)

    def wave(ref, w):
        off, count = waves[w]
        return lambda c, i: ref.at[c, i, :, :, pl.ds(off, count)]

    def wave_rings(w):
        off, count = waves[w]
        for ref, i in ((a_gu, xi), (b_gu, zi)):
            forward(fwd_gu[w], lambda c: wave(ref, w)(c, i))
        return (
            Ring("x", lambda i, h: a_gu.at[ci, i, two(h), :, pl.ds(off, count)]),
            Ring("z", lambda i, h: b_gu.at[ci, i, two(h), :, pl.ds(off, count)]),
        )

    def done(waits):
        for w in waits:
            w()

    def forward(keep, ref_of):
        keep.append(push("c", 1, ref_of(ci), ref_of(1 - ci)))

    def group(ref):
        return lambda c, i: ref.at[c, i]

    def finish_near(ring, keep, of, i):
        ring.near()
        forward(keep, lambda c: of(c, wrap(i, -1)))
        forward(keep, lambda c: of(c, wrap(i, 1)))

    def finish_far(ring, keep, of, i):
        ring.end()
        forward(keep, lambda c: of(c, wrap(i, 2)))

    fwd_v, fwd_g, fwd_o, fwd_gu = [], [], [], [[], [], []]
    done(own_gu)
    first = (Ring("z", lambda i, h: a_gu.at[ci, xi, i, h]),
             Ring("x", lambda i, h: b_gu.at[ci, zi, i, h]))
    done(v1)
    v2 = direct("x", lambda i: vw.at[ci, yi, i], None)
    done(g1)
    g2 = direct("z", lambda i: gw.at[ci, xi, i], lambda i, h: gw.at[ci, xi, i, two(h)])
    done(o1)
    o2 = direct("y", lambda i: ow.at[ci, zi, i], None)
    for ring in first:
        ring.relay()
    done(v2)
    v3 = Ring("y", lambda i, h: vw.at[ci, i, two(h)])
    forward(fwd_v, lambda c: vw.at[c, yi])
    done(g2)
    g3 = Ring("x", lambda i, h: gw.at[ci, i, two(h)])
    forward(fwd_g, lambda c: gw.at[c, xi])
    done(o2)
    o3 = Ring("z", lambda i, h: ow.at[ci, i, two(h)])
    forward(fwd_o, lambda c: ow.at[c, zi])

    got_tok()
    done(got_small)
    floats = tok[...].astype(F32)
    scale = lax.rsqrt(jnp.mean(floats * floats, axis=-1, keepdims=True) + EPS)
    nbuf[...] = (floats * scale * row(gain1)).astype(BF)

    v3.relay()
    g3.relay()
    o3.relay()
    for ring in first:
        ring.near()
        ring.end()
    second = [wave_rings(w) for w in range(len(waves))]
    done(own_d)
    ad1 = Ring("z", lambda i, h: a_d.at[ci, xi, i, pl.ds(h * hr, hr)])
    bd1 = Ring("x", lambda i, h: b_d.at[ci, zi, i, pl.ds(h * hr, hr)])
    finish_near(v3, fwd_v, group(vw), yi)
    finish_far(v3, fwd_v, group(vw), yi)
    finish_near(g3, fwd_g, group(gw), xi)
    finish_near(o3, fwd_o, group(ow), zi)
    finish_far(g3, fwd_g, group(gw), xi)
    done(fwd_v)

    every = [(z, x) for z in range(N) for x in range(N)]

    def project(block, lo):
        cols = [
            cat([block(c, y, z, x) for y in (lo, lo + 1) for c in range(2)], 0) for z, x in every
        ]
        return dot_nt(nbuf[...], cat(cols, 1))

    width = 512
    activated = gelu(cat([project(lambda c, y, z, x: vw[c, y, x, z], lo) for lo in (0, 2)], 1))
    center = jnp.sum(activated, axis=-1, keepdims=True) / width
    spread = jnp.sum(activated * activated, axis=-1, keepdims=True) / width - center * center
    values = (
        (activated - center) * lax.rsqrt(spread + EPS) * row(lgain) + row(lshift)
    ).astype(BF)
    finish_far(o3, fwd_o, group(ow), zi)
    span, groups = mixk.shape[1], mixk.shape[0]
    t_pos = lax.broadcasted_iota(jnp.int32, (span, span), 0)
    s_pos = lax.broadcasted_iota(jnp.int32, (span, span), 1)
    mixing = []
    for g in range(groups):
        masked = jnp.where(s_pos <= t_pos, mixk[g].astype(F32), 0.0).astype(BF)
        offset_row = mixo[g : g + 1, :].astype(F32)
        offset = jnp.sum(jnp.where(s_pos == t_pos, offset_row, 0.0), axis=-1, keepdims=True)
        mixing.append(
            jnp.dot(masked, values[:, g * span : (g + 1) * span], preferred_element_type=F32)
            + offset
        )
    done(fwd_g)
    gate_u = gelu(cat([project(lambda c, y, z, x: gw[c, x, z, y], lo) for lo in (0, 2)], 1))
    gated = (gate_u * cat(mixing, 1)).astype(BF)
    done(fwd_o)
    total = jnp.zeros((span, 1), F32)
    lane = 128
    for z in range(N):
        weights = cat(
            [
                cat([ow[c, z, y, x] for y in range(N) for c in range(2)], 0)
                for x in range(N)
            ],
            1,
        )
        cols = slice(z * N * lane, (z + 1) * N * lane)
        mid = (
            tok[:, cols].astype(F32) + jnp.dot(gated, weights, preferred_element_type=F32)
        ).astype(BF)
        middle[:, cols] = mid
        mid = mid.astype(F32)
        total += jnp.sum(mid * mid, axis=-1, keepdims=True)
    width2 = middle.shape[1]
    scale2 = lax.rsqrt(total / width2 + EPS)
    xall[yi] = (middle[...].astype(F32) * scale2 * row(gain2)).astype(BF)

    toks = Ring("y", lambda i, h: xall.at[i, pl.ds(h * (span // 2), span // 2)])

    order = [zi, wrap(zi, -1), wrap(zi, 1), wrap(zi, 2)]
    before, after, far = wrap(xi, -1), wrap(xi, 1), wrap(xi, 2)
    ad2, ad2_last = [], []

    def down_send(k):
        z = order[k]
        ad2.append([push("x", 1, a_d.at[ci, xi, z], a_d.at[ci, before, z]),
                    push("x", -1, a_d.at[ci, xi, z], a_d.at[ci, after, z])])

    def down_relay(k):
        z = order[k]
        ad2[k][0]()
        up = push("x", 1, a_d.at[ci, before, z, pl.ds(0, hr)], a_d.at[ci, far, z, pl.ds(0, hr)])
        ad2[k][1]()
        down = push(
            "x", -1, a_d.at[ci, after, z, pl.ds(hr, hr)], a_d.at[ci, far, z, pl.ds(hr, hr)]
        )
        ad2_last.append([up, down])

    def finish_wave(w):
        for finish in (finish_near, finish_far):
            finish(second[w][0], fwd_gu[w], wave(a_gu, w), xi)
            finish(second[w][1], fwd_gu[w], wave(b_gu, w), zi)

    for ring in second[0]:
        ring.relay()
    for ring in second[1]:
        ring.relay()
    toks.relay()
    for ring in second[2]:
        ring.relay()
    for ring in (ad1, bd1):
        ring.relay()
    down_send(0)
    for ring in (ad1, bd1):
        ring.near()
    down_send(1)
    down_send(2)
    finish_wave(0)
    finish_wave(1)
    toks.near()
    toks.end()
    done(fwd_gu[0])

    def unit_rows(w, which, lo, hi):
        count = waves[w][1]
        pieces = []
        for seg in range(4):
            a, b = max(lo, seg * count), min(hi, (seg + 1) * count)
            if a < b:
                c, h = divmod(seg, 2)
                r = slice(waves[w][0] + a - seg * count, waves[w][0] + b - seg * count)
                ref = (a_gu, b_gu)[h]
                pieces.append(
                    cat(
                        [
                            ref[(c, x, z) + (which, r)] if h == 0 else ref[(c, z, x) + (which, r)]
                            for z, x in every
                        ],
                        1,
                    )
                )
        return cat(pieces, 0)

    rows_all = xall.reshape(N * span, width2)
    step = 256

    def hidden_tile(w, lo):
        count = 4 * waves[w][1]
        hi = min(lo + step, count)
        if hi - lo == step:
            gate_pre = dot_nt(rows_all[...], unit_rows(w, 0, lo, hi))
            up_pre = dot_nt(rows_all[...], unit_rows(w, 1, lo, hi))
        else:
            both = dot_nt(
                rows_all[...], cat([unit_rows(w, 0, lo, hi), unit_rows(w, 1, lo, hi)], 0)
            )
            gate_pre, up_pre = both[:, : hi - lo], both[:, hi - lo :]
        at = 4 * waves[w][0]
        hidden[:, at + lo : at + hi] = (gate_pre * lax.logistic(gate_pre) * up_pre).astype(BF)

    for lo in range(0, 4 * waves[0][1], step):
        hidden_tile(0, lo)
    for ring in (ad1, bd1):
        ring.end()
    bd2 = Ring("z", lambda i, h: b_d.at[ci, i, two(h)])
    down_send(3)
    finish_wave(2)
    done(fwd_gu[1])
    hidden_tile(1, 0)
    down_relay(0)
    hidden_tile(1, step)
    done(fwd_gu[2])
    hidden_tile(2, 0)
    fwd_d = []

    def down_forward(k):
        z = order[k]
        if k == 1:
            bd2.relay()
            bd2.near()
        if k == 3:
            bd2.end()
        for w in ad2_last[k]:
            w()
        fwd = []
        forward(fwd, lambda c: a_d.at[c, :, z])
        forward(fwd, lambda c: b_d.at[c, z])
        fwd_d.append(fwd)

    down_forward(0)
    hidden_tile(2, step)
    down_relay(1)

    got_r1, got_r2, ahead, back = {}, {}, wrap(yi, 1), wrap(yi, -1)
    opposite = wrap(yi, 2)

    def sum_first(r):
        z, lo, mid, hi = rounds[r]
        low, high = pl.ds(lo, mid - lo), pl.ds(mid, hi - mid)
        got_r1[r] = [
            send_to("y", 1, parts.at[opposite, z, low], r1.at[0, z, low]),
            send_to("y", -1, parts.at[opposite, z, high], r1.at[1, z, high]),
        ]
        got_r2[r] = [
            send_to("y", 1, parts.at[ahead, z, high], r2.at[0, z, high]),
            send_to("y", -1, parts.at[back, z, low], r2.at[1, z, low]),
        ]

    def send_to(axis, s, src, dst):
        k = len(sends)
        copy = pltpu.make_async_remote_copy(
            src, dst, ssem.at[k], rsem.at[k], device_id=device(axis, s),
            device_id_type=pl.DeviceIdType.MESH,
        )
        copy.start()
        sends.append(copy)
        return copy.wait_recv

    def sum_second(r):
        z, lo, mid, hi = rounds[r]
        low, high = pl.ds(lo, mid - lo), pl.ds(mid, hi - mid)
        got_r1[r][0]()
        parts[ahead, z, low] = (
            parts[ahead, z, low].astype(F32) + r1[0, z, low].astype(F32)
        ).astype(BF)
        got_r2[r].append(send_to("y", 1, parts.at[ahead, z, low], r2.at[0, z, low]))
        got_r1[r][1]()
        parts[back, z, high] = (
            parts[back, z, high].astype(F32) + r1[1, z, high].astype(F32)
        ).astype(BF)
        got_r2[r].append(send_to("y", -1, parts.at[back, z, high], r2.at[1, z, high]))

    def sum_last(r):
        z, lo, mid, hi = rounds[r]
        done(got_r2[r])
        for x in range(lo, hi):
            summed = (
                parts[yi, z, x].astype(F32) + r2[0, z, x].astype(F32) + r2[1, z, x].astype(F32)
            )
            cols = pl.ds(pl.multiple_of((z * N + x) * lane, lane), lane)
            out[:, cols] = (middle[:, cols].astype(F32) + summed).astype(BF)

    def multiply(z, x2):
        weights = cat(
            [
                cat(
                    [
                        ref
                        for off, count in waves
                        for c in range(2)
                        for ref in (a_d[c, x, z, off : off + count], b_d[c, z, x, off : off + count])
                    ],
                    0,
                )
                for x in (x2, x2 + 1)
            ],
            1,
        )
        result = jnp.dot(hidden[...], weights, preferred_element_type=F32).astype(BF)
        for y in range(N):
            for j in range(2):
                parts[y, z, x2 + j] = result[y * span : (y + 1) * span, j * lane : (j + 1) * lane]

    rounds = [(order[0], 0, 2, 4), (order[1], 0, 2, 4), (order[2], 0, 2, 4),
              (order[3], 0, 1, 2), (order[3], 2, 3, 4)]
    for k in range(N - 1):
        done(fwd_d[k])
        multiply(order[k], 0)
        multiply(order[k], 2)
        sum_first(k)
        down_forward(k + 1)
        if k + 2 < N:
            down_relay(k + 2)
        if k:
            sum_second(k - 1)
    done(fwd_d[3])
    multiply(order[3], 0)
    sum_first(3)
    multiply(order[3], 2)
    sum_first(4)
    sum_second(2)
    sum_last(0)
    sum_second(3)
    sum_second(4)
    sum_last(1)
    sum_last(2)
    sum_last(3)
    sum_last(4)
    assert len(sends) <= COPIES
    for copy in sends:
        copy.wait_send()


def per_device(
    tokens, mix_gain, gate_proj, value_proj, layer_gain, layer_shift, mix_kernel, mix_offset,
    out_proj, ffn_gain, ffn_gate, ffn_up, ffn_down,
):
    span, width = tokens.shape
    units, lane = ffn_gate.shape[1], ffn_gate.shape[0]
    local = gate_proj.shape[1]
    half = units // 2
    anywhere = pl.BlockSpec(memory_space=pl.ANY)
    return pl.pallas_call(
        kernel,
        out_shape=jax.ShapeDtypeStruct(tokens.shape, BF),
        in_specs=[anywhere] * 13,
        out_specs=pl.BlockSpec(memory_space=pltpu.VMEM),
        scratch_shapes=[
            pltpu.VMEM((span, width), BF),
            pltpu.VMEM(mix_gain.shape, BF),
            pltpu.VMEM(ffn_gain.shape, BF),
            pltpu.VMEM(layer_gain.shape, BF),
            pltpu.VMEM(layer_shift.shape, BF),
            pltpu.VMEM(mix_offset.shape, BF),
            pltpu.VMEM(mix_kernel.shape, BF),
            pltpu.VMEM((2, N, N, N, local, lane), BF),
            pltpu.VMEM((2, N, N, N, local, lane), BF),
            pltpu.VMEM((2, N, N, N, local, lane), BF),
            pltpu.VMEM((2, N, N, 2, half, lane), BF),
            pltpu.VMEM((2, N, N, 2, half, lane), BF),
            pltpu.VMEM((2, N, N, half, lane), BF),
            pltpu.VMEM((2, N, N, half, lane), BF),
            pltpu.VMEM((span, width), BF),
            pltpu.VMEM((span, width), BF),
            pltpu.VMEM((N, span, width), BF),
            pltpu.VMEM((N * span, 2 * units), BF),
            pltpu.VMEM((N, N, N, span, lane), BF),
            pltpu.VMEM((2, N, N, span, lane), BF),
            pltpu.VMEM((2, N, N, span, lane), BF),
            pltpu.SemaphoreType.DMA((24,)),
            pltpu.SemaphoreType.DMA((COPIES,)),
            pltpu.SemaphoreType.DMA((COPIES,)),
        ],
        compiler_params=pltpu.CompilerParams(
            collective_id=0, has_side_effects=True, vmem_limit_bytes=63 * 2**20
        ),
    )(
        tokens, gate_proj.T, value_proj.T, out_proj.T, ffn_gate.T, ffn_up.T, ffn_down.T,
        mix_gain, layer_gain, layer_shift, mix_kernel, mix_offset, ffn_gain,
    )


def solution(mesh):
    torus = Mesh(mesh.devices.reshape(mesh.shape["rep"], 4, 4, 4, 2), AXES)
    return jax.shard_map(
        per_device,
        mesh=torus,
        in_specs=(
            P(AXES, None), P(), P(FS, TP), P(FS, TP), P(), P(), P(), P(), P(FS, TP), P(),
            P(FS, TP), P(FS, TP), P(FS, TP),
        ),
        out_specs=P(AXES, None),
        check_vma=False,
    )
```

time: 107 us -> 95.4 us (0.89)
  Pallas kernels: 102 us -> 93.4 us
  local copies, waits for them, and re-layouts: 4.03 us -> 1.88 us
    pallas_call x1, Pallas kernels: 102 us -> 93.4 us  [per_device(): pl.pallas_call(kernel, out_shape=jax.ShapeDtypeStruct(tokens.shape, BF),...]
    unnamed x11 -> x1, local copies, waits for them, and re-layouts: 3.92 us -> 1.88 us
where the time goes in v2:
time: 95.4 us; the launch traced here: 95.3 us
  Pallas kernels  93.4 us (98%)
  local copies, waits for them, and re-layouts  1.88 us (2%)
    pallas_call x1, Pallas kernels, per_device(): pl.pallas_call(kernel, out_shape=jax.ShapeDtypeStruct(tokens.shape, BF),...  93.4 us

profile of v2, /device:TPU:1, one launch (start us, length us, event | category | flops | bytes accessed | tf_op | source)
XLA Modules:
  0.0 95.3 jit_solution(17180190209006581726)
XLA Ops:
  0.0 93.4 %shard_map.127 = bf16[128,2048]{1,0:T(8,128)(2,1)} custom-call(bf16[128,2048]{1,0:T(8,128)(2,1)} %tokens.1, bf16[64,128]{1,0:T(8,128)(2,1)} %bitcast.9, bf16[64,128]{1,0:T(8,128)(2,1)} %bitcast.10, bf16[64,128]{1,0:T(8,128)(2,1)} %bitcast.11, bf16[704,128]{1,0:T(8,128)(2,1)} %bitcast.6, bf16[704,128]{1,0:T(8,128)(2,1)} %bitcast.7, bf16[704,128]{1,0:T(8,128)(2,1)} %bitcast.8, ...), custom_call_target="tpu_custom_call" | custom-call | tf_op jit(solution)/shard_map/pallas_call | solution.py:530
  93.4 1.9 %copy.15 = bf16[128,2048]{1,0:T(8,128)(2,1)} copy(bf16[128,2048]{1,0:T(8,128)(2,1)} %shard_map.127) | data formatting | bytes 1048576

commit v3 on v2

--- a/solution.py
+++ b/solution.py
@@ -88,8 +88,6 @@
     half = a_d.shape[-2]
     hr = half // 2
     waves = row_waves(half)
-    half = a_d.shape[-2]
-    hr = half // 2
     own_v = load(value_proj, vw.at[ci, yi, xi, zi])
     own_g = load(gate_proj, gw.at[ci, xi, zi, yi])
     own_o = load(out_proj, ow.at[ci, zi, yi, xi])
@@ -238,15 +236,11 @@
     for ring in first:
         ring.near()
         ring.end()
-    second = [wave_rings(w) for w in range(len(waves))]
-    done(own_d)
-    ad1 = Ring("z", lambda i, h: a_d.at[ci, xi, i, pl.ds(h * hr, hr)])
-    bd1 = Ring("x", lambda i, h: b_d.at[ci, zi, i, pl.ds(h * hr, hr)])
+    second = [wave_rings(0), wave_rings(1)]
     finish_near(v3, fwd_v, group(vw), yi)
     finish_far(v3, fwd_v, group(vw), yi)
     finish_near(g3, fwd_g, group(gw), xi)
     finish_near(o3, fwd_o, group(ow), zi)
-    finish_far(g3, fwd_g, group(gw), xi)
     done(fwd_v)
 
     every = [(z, x) for z in range(N) for x in range(N)]
@@ -264,6 +258,7 @@
     values = (
         (activated - center) * lax.rsqrt(spread + EPS) * row(lgain) + row(lshift)
     ).astype(BF)
+    finish_far(g3, fwd_g, group(gw), xi)
     finish_far(o3, fwd_o, group(ow), zi)
     span, groups = mixk.shape[1], mixk.shape[0]
     t_pos = lax.broadcasted_iota(jnp.int32, (span, span), 0)
@@ -306,12 +301,12 @@
 
     order = [zi, wrap(zi, -1), wrap(zi, 1), wrap(zi, 2)]
     before, after, far = wrap(xi, -1), wrap(xi, 1), wrap(xi, 2)
-    ad2, ad2_last = [], []
+    ad2, ad2_last = {}, {}
 
     def down_send(k):
         z = order[k]
-        ad2.append([push("x", 1, a_d.at[ci, xi, z], a_d.at[ci, before, z]),
-                    push("x", -1, a_d.at[ci, xi, z], a_d.at[ci, after, z])])
+        ad2[k] = [push("x", 1, a_d.at[ci, xi, z], a_d.at[ci, before, z]),
+                  push("x", -1, a_d.at[ci, xi, z], a_d.at[ci, after, z])]
 
     def down_relay(k):
         z = order[k]
@@ -321,7 +316,7 @@
         down = push(
             "x", -1, a_d.at[ci, after, z, pl.ds(hr, hr)], a_d.at[ci, far, z, pl.ds(hr, hr)]
         )
-        ad2_last.append([up, down])
+        ad2_last[k] = [up, down]
 
     def finish_wave(w):
         for finish in (finish_near, finish_far):
@@ -330,22 +325,18 @@
 
     for ring in second[0]:
         ring.relay()
+    done(own_d)
+    ad1 = Ring("z", lambda i, h: a_d.at[ci, xi, i, pl.ds(h * hr, hr)])
+    bd1 = Ring("x", lambda i, h: b_d.at[ci, zi, i, pl.ds(h * hr, hr)])
     for ring in second[1]:
         ring.relay()
+    second.append(wave_rings(2))
     toks.relay()
-    for ring in second[2]:
-        ring.relay()
+    finish_wave(0)
     for ring in (ad1, bd1):
         ring.relay()
-    down_send(0)
-    for ring in (ad1, bd1):
-        ring.near()
-    down_send(1)
-    down_send(2)
-    finish_wave(0)
     finish_wave(1)
     toks.near()
-    toks.end()
     done(fwd_gu[0])
 
     def unit_rows(w, which, lo, hi):
@@ -368,66 +359,88 @@
                 )
         return cat(pieces, 0)
 
-    rows_all = xall.reshape(N * span, width2)
     step = 256
-
-    def hidden_tile(w, lo):
+    places = [yi, wrap(yi, -1), wrap(yi, 1), wrap(yi, 2)]
+
+    def hidden_tile(w, lo, first, last):
         count = 4 * waves[w][1]
         hi = min(lo + step, count)
+        block = cat([xall[y] for y in places[first:last]], 0)
         if hi - lo == step:
-            gate_pre = dot_nt(rows_all[...], unit_rows(w, 0, lo, hi))
-            up_pre = dot_nt(rows_all[...], unit_rows(w, 1, lo, hi))
+            gate_pre = dot_nt(block, unit_rows(w, 0, lo, hi))
+            up_pre = dot_nt(block, unit_rows(w, 1, lo, hi))
         else:
-            both = dot_nt(
-                rows_all[...], cat([unit_rows(w, 0, lo, hi), unit_rows(w, 1, lo, hi)], 0)
-            )
+            weights = cat([unit_rows(w, 0, lo, hi), unit_rows(w, 1, lo, hi)], 0)
+            middle_row = block.shape[0] // 2
+            both = cat([dot_nt(b, weights) for b in (block[:middle_row], block[middle_row:])], 0)
             gate_pre, up_pre = both[:, : hi - lo], both[:, hi - lo :]
         at = 4 * waves[w][0]
-        hidden[:, at + lo : at + hi] = (gate_pre * lax.logistic(gate_pre) * up_pre).astype(BF)
-
-    for lo in range(0, 4 * waves[0][1], step):
-        hidden_tile(0, lo)
+        hidden[first * span : last * span, at + lo : at + hi] = (
+            gate_pre * lax.logistic(gate_pre) * up_pre
+        ).astype(BF)
+
+    hidden_tile(0, 0, 0, 3)
+    hidden_tile(0, step, 0, 3)
+    for ring in second[2]:
+        ring.relay()
+    down_send(0)
+    done(fwd_gu[1])
+    hidden_tile(1, 0, 0, 3)
+    hidden_tile(1, step, 0, 3)
+    for ring in (ad1, bd1):
+        ring.near()
+    down_send(1)
     for ring in (ad1, bd1):
         ring.end()
     bd2 = Ring("z", lambda i, h: b_d.at[ci, i, two(h)])
+    fwd_d = [[] for _ in range(N + 1)]
+    forward(fwd_d[0], lambda c: a_d.at[c, xi, zi])
+    forward(fwd_d[0], lambda c: b_d.at[c, zi])
+    toks.end()
+    hidden_tile(0, 0, 3, 4)
+    hidden_tile(0, step, 3, 4)
+    finish_wave(2)
+    hidden_tile(1, 0, 3, 4)
+    hidden_tile(1, step, 3, 4)
+    down_relay(0)
+    down_send(2)
+    forward(fwd_d[0], lambda c: a_d.at[c, wrap(xi, -1), zi])
+    forward(fwd_d[1], lambda c: a_d.at[c, wrap(xi, 1), zi])
+    done(fwd_gu[2])
+    hidden_tile(2, 0, 0, 4)
+    down_relay(1)
     down_send(3)
-    finish_wave(2)
-    done(fwd_gu[1])
-    hidden_tile(1, 0)
-    down_relay(0)
-    hidden_tile(1, step)
-    done(fwd_gu[2])
-    hidden_tile(2, 0)
-    fwd_d = []
+    bd2.relay()
+    hidden_tile(2, step, 0, 4)
 
     def down_forward(k):
         z = order[k]
-        if k == 1:
-            bd2.relay()
-            bd2.near()
-        if k == 3:
-            bd2.end()
-        for w in ad2_last[k]:
-            w()
-        fwd = []
-        forward(fwd, lambda c: a_d.at[c, :, z])
-        forward(fwd, lambda c: b_d.at[c, z])
-        fwd_d.append(fwd)
-
-    down_forward(0)
-    hidden_tile(2, step)
-    down_relay(1)
-
-    got_r1, got_r2, ahead, back = {}, {}, wrap(yi, 1), wrap(yi, -1)
-    opposite = wrap(yi, 2)
+        done(ad2_last[k])
+        forward(fwd_d[k + 1], lambda c: a_d.at[c, :, z])
+        forward(fwd_d[k + 1], lambda c: b_d.at[c, z])
+
+    got_r1, got_r2 = {}, {}
+    own, back, ahead, opposite = range(N)
+
+    pairs = (pl.ds(0, 2), pl.ds(2, 2))
+    rounds = [
+        (order[0], xi, before, (xi, before)),
+        (order[0], after, far, (after, far)),
+        (order[1], *pairs, range(N)),
+        (order[2], *pairs, range(N)),
+        (order[3], 0, 1, (0, 1)),
+        (order[3], 2, 3, (2, 3)),
+    ]
 
     def sum_first(r):
-        z, lo, mid, hi = rounds[r]
-        low, high = pl.ds(lo, mid - lo), pl.ds(mid, hi - mid)
+        z, low, high, _ = rounds[r]
         got_r1[r] = [
             send_to("y", 1, parts.at[opposite, z, low], r1.at[0, z, low]),
             send_to("y", -1, parts.at[opposite, z, high], r1.at[1, z, high]),
         ]
+
+    def sum_direct(r):
+        z, low, high, _ = rounds[r]
         got_r2[r] = [
             send_to("y", 1, parts.at[ahead, z, high], r2.at[0, z, high]),
             send_to("y", -1, parts.at[back, z, low], r2.at[1, z, low]),
@@ -444,8 +457,7 @@
         return copy.wait_recv
 
     def sum_second(r):
-        z, lo, mid, hi = rounds[r]
-        low, high = pl.ds(lo, mid - lo), pl.ds(mid, hi - mid)
+        z, low, high, _ = rounds[r]
         got_r1[r][0]()
         parts[ahead, z, low] = (
             parts[ahead, z, low].astype(F32) + r1[0, z, low].astype(F32)
@@ -458,16 +470,16 @@
         got_r2[r].append(send_to("y", -1, parts.at[back, z, high], r2.at[1, z, high]))
 
     def sum_last(r):
-        z, lo, mid, hi = rounds[r]
+        z, _, _, blocks = rounds[r]
         done(got_r2[r])
-        for x in range(lo, hi):
+        for x in blocks:
             summed = (
-                parts[yi, z, x].astype(F32) + r2[0, z, x].astype(F32) + r2[1, z, x].astype(F32)
+                parts[own, z, x].astype(F32) + r2[0, z, x].astype(F32) + r2[1, z, x].astype(F32)
             )
             cols = pl.ds(pl.multiple_of((z * N + x) * lane, lane), lane)
             out[:, cols] = (middle[:, cols].astype(F32) + summed).astype(BF)
 
-    def multiply(z, x2):
+    def multiply(z, xs):
         weights = cat(
             [
                 cat(
@@ -479,40 +491,65 @@
                     ],
                     0,
                 )
-                for x in (x2, x2 + 1)
+                for x in xs
             ],
             1,
         )
-        result = jnp.dot(hidden[...], weights, preferred_element_type=F32).astype(BF)
-        for y in range(N):
-            for j in range(2):
-                parts[y, z, x2 + j] = result[y * span : (y + 1) * span, j * lane : (j + 1) * lane]
-
-    rounds = [(order[0], 0, 2, 4), (order[1], 0, 2, 4), (order[2], 0, 2, 4),
-              (order[3], 0, 1, 2), (order[3], 2, 3, 4)]
-    for k in range(N - 1):
-        done(fwd_d[k])
-        multiply(order[k], 0)
-        multiply(order[k], 2)
-        sum_first(k)
-        down_forward(k + 1)
-        if k + 2 < N:
-            down_relay(k + 2)
-        if k:
-            sum_second(k - 1)
+        for y in range(0, N, 2):
+            rows_y = hidden[y * span : (y + 2) * span, :]
+            result = jnp.dot(rows_y, weights, preferred_element_type=F32).astype(BF)
+            for i in range(2):
+                for j, x in enumerate(xs):
+                    parts[y + i, z, x] = result[
+                        i * span : (i + 1) * span, j * lane : (j + 1) * lane
+                    ]
+
+    done(fwd_d[0])
+    multiply(order[0], (xi, before))
+    sum_first(0)
+    sum_direct(0)
+    done(ad2_last[0])
+    forward(fwd_d[1], lambda c: a_d.at[c, wrap(xi, 2), zi])
+    down_relay(2)
+    bd2.near()
+    down_forward(1)
+    done(fwd_d[1])
+    multiply(order[0], (after, far))
+    sum_first(1)
+    sum_direct(1)
+    sum_second(0)
+    done(fwd_d[2])
+    multiply(order[1], (0, 1))
+    multiply(order[1], (2, 3))
+    sum_first(2)
+    sum_direct(2)
+    down_relay(3)
+    down_forward(2)
+    sum_second(1)
     done(fwd_d[3])
-    multiply(order[3], 0)
+    multiply(order[2], (0, 1))
+    multiply(order[2], (2, 3))
     sum_first(3)
-    multiply(order[3], 2)
+    sum_direct(3)
+    bd2.end()
+    down_forward(3)
+    sum_second(2)
+    done(fwd_d[4])
+    multiply(order[3], (0, 1))
     sum_first(4)
-    sum_second(2)
+    multiply(order[3], (2, 3))
+    sum_first(5)
+    sum_direct(4)
+    sum_direct(5)
+    sum_second(3)
     sum_last(0)
-    sum_second(3)
+    sum_last(1)
     sum_second(4)
-    sum_last(1)
+    sum_second(5)
     sum_last(2)
     sum_last(3)
     sum_last(4)
+    sum_last(5)
     assert len(sends) <= COPIES
     for copy in sends:
         copy.wait_send()

time: 95.4 us -> 91 us (0.954)
  Pallas kernels: 93.4 us -> 89 us
    pallas_call x1, Pallas kernels: 93.4 us -> 89 us  [per_device(): pl.pallas_call(kernel, out_shape=jax.ShapeDtypeStruct(tokens.shape, BF),...]
where the time goes in v3:
time: 91 us; the launch traced here: 90.9 us
  Pallas kernels  89 us (98%)
  local copies, waits for them, and re-layouts  1.88 us (2%)
    pallas_call x1, Pallas kernels, per_device(): pl.pallas_call(kernel, out_shape=jax.ShapeDtypeStruct(tokens.shape, BF),...  89 us
    unnamed x1, local copies, waits for them, and re-layouts  1.88 us

profile of v3, /device:TPU:1, one launch (start us, length us, event | category | flops | bytes accessed | tf_op | source)
XLA Modules:
  0.0 90.9 jit_solution(9532672041027119110)
XLA Ops:
  0.0 89.0 %shard_map.127 = bf16[128,2048]{1,0:T(8,128)(2,1)} custom-call(bf16[128,2048]{1,0:T(8,128)(2,1)} %tokens.1, bf16[64,128]{1,0:T(8,128)(2,1)} %bitcast.9, bf16[64,128]{1,0:T(8,128)(2,1)} %bitcast.10, bf16[64,128]{1,0:T(8,128)(2,1)} %bitcast.11, bf16[704,128]{1,0:T(8,128)(2,1)} %bitcast.6, bf16[704,128]{1,0:T(8,128)(2,1)} %bitcast.7, bf16[704,128]{1,0:T(8,128)(2,1)} %bitcast.8, ...), custom_call_target="tpu_custom_call" | custom-call | tf_op jit(solution)/shard_map/pallas_call | solution.py:567
  89.0 1.9 %copy.15 = bf16[128,2048]{1,0:T(8,128)(2,1)} copy(bf16[128,2048]{1,0:T(8,128)(2,1)} %shard_map.127) | data formatting | bytes 1048576

commit v4 on v3

--- a/solution.py
+++ b/solution.py
@@ -13,7 +13,7 @@
 TP = ("tp_0", "tp_1")
 EPS = 1e-06
 N = 4
-COPIES = 216
+COPIES = 272
 
 
 def row_waves(half):
@@ -299,29 +299,52 @@
 
     toks = Ring("y", lambda i, h: xall.at[i, pl.ds(h * (span // 2), span // 2)])
 
-    order = [zi, wrap(zi, -1), wrap(zi, 1), wrap(zi, 2)]
-    before, after, far = wrap(xi, -1), wrap(xi, 1), wrap(xi, 2)
-    ad2, ad2_last = {}, {}
+    places_x = [xi, wrap(xi, -1), wrap(xi, 1), wrap(xi, 2)]
+    places_z = [zi, wrap(zi, -1), wrap(zi, 1), wrap(zi, 2)]
+    got_near, got_far = {}, {}
+    fwd_d = [[] for _ in range(8)]
+
+    def block_a(c, x, z, at=pl.ds(0, half)):
+        return a_d.at[c, x, z, at]
+
+    def block_b(c, z, x, at=pl.ds(0, half)):
+        return b_d.at[c, z, x, at]
+
+    lines = (("x", block_a, places_x, places_z), ("z", block_b, places_z, places_x))
 
     def down_send(k):
-        z = order[k]
-        ad2[k] = [push("x", 1, a_d.at[ci, xi, z], a_d.at[ci, before, z]),
-                  push("x", -1, a_d.at[ci, xi, z], a_d.at[ci, after, z])]
-
-    def down_relay(k):
-        z = order[k]
-        ad2[k][0]()
-        up = push("x", 1, a_d.at[ci, before, z, pl.ds(0, hr)], a_d.at[ci, far, z, pl.ds(0, hr)])
-        ad2[k][1]()
-        down = push(
-            "x", -1, a_d.at[ci, after, z, pl.ds(hr, hr)], a_d.at[ci, far, z, pl.ds(hr, hr)]
-        )
-        ad2_last[k] = [up, down]
-
-    def finish_wave(w):
-        for finish in (finish_near, finish_far):
-            finish(second[w][0], fwd_gu[w], wave(a_gu, w), xi)
-            finish(second[w][1], fwd_gu[w], wave(b_gu, w), zi)
+        for axis, block, along, other in lines:
+            mine = block(ci, along[0], other[k])
+            got_near[axis, k] = [push(axis, 1, mine, block(ci, along[1], other[k])),
+                                 push(axis, -1, mine, block(ci, along[2], other[k]))]
+
+    def down_near(k):
+        for axis, block, along, other in lines:
+            got_far[axis, k] = []
+            for h, (w, s, j) in enumerate(zip(got_near[axis, k], (1, -1), (1, 2))):
+                w()
+                at = pl.ds(h * hr, hr)
+                got_far[axis, k].append(
+                    push(axis, s, block(ci, along[j], other[k], at), block(ci, along[3], other[k], at))
+                )
+
+    def down_near_forward(f, k):
+        for axis, block, along, other in lines:
+            for j in (1, 2):
+                forward(fwd_d[f], lambda c: block(c, along[j], other[k]))
+
+    def down_far_forward(f, k):
+        for axis, block, along, other in lines:
+            done(got_far[axis, k])
+            forward(fwd_d[f], lambda c: block(c, along[3], other[k]))
+
+    def near_wave(w):
+        finish_near(second[w][0], fwd_gu[w], wave(a_gu, w), xi)
+        finish_near(second[w][1], fwd_gu[w], wave(b_gu, w), zi)
+
+    def far_wave(w):
+        finish_far(second[w][0], fwd_gu[w], wave(a_gu, w), xi)
+        finish_far(second[w][1], fwd_gu[w], wave(b_gu, w), zi)
 
     for ring in second[0]:
         ring.relay()
@@ -331,11 +354,12 @@
     for ring in second[1]:
         ring.relay()
     second.append(wave_rings(2))
+    near_wave(0)
     toks.relay()
-    finish_wave(0)
+    far_wave(0)
     for ring in (ad1, bd1):
         ring.relay()
-    finish_wave(1)
+    near_wave(1)
     toks.near()
     done(fwd_gu[0])
 
@@ -381,69 +405,55 @@
 
     hidden_tile(0, 0, 0, 3)
     hidden_tile(0, step, 0, 3)
+    far_wave(1)
     for ring in second[2]:
         ring.relay()
     down_send(0)
     done(fwd_gu[1])
     hidden_tile(1, 0, 0, 3)
     hidden_tile(1, step, 0, 3)
+    near_wave(2)
     for ring in (ad1, bd1):
         ring.near()
     down_send(1)
+    down_send(2)
     for ring in (ad1, bd1):
         ring.end()
-    bd2 = Ring("z", lambda i, h: b_d.at[ci, i, two(h)])
-    fwd_d = [[] for _ in range(N + 1)]
-    forward(fwd_d[0], lambda c: a_d.at[c, xi, zi])
+    forward(fwd_d[0], lambda c: a_d.at[c, xi])
     forward(fwd_d[0], lambda c: b_d.at[c, zi])
     toks.end()
     hidden_tile(0, 0, 3, 4)
     hidden_tile(0, step, 3, 4)
-    finish_wave(2)
+    far_wave(2)
     hidden_tile(1, 0, 3, 4)
     hidden_tile(1, step, 3, 4)
-    down_relay(0)
-    down_send(2)
-    forward(fwd_d[0], lambda c: a_d.at[c, wrap(xi, -1), zi])
-    forward(fwd_d[1], lambda c: a_d.at[c, wrap(xi, 1), zi])
+    down_near(0)
+    down_near_forward(1, 0)
+    down_send(3)
     done(fwd_gu[2])
     hidden_tile(2, 0, 0, 4)
-    down_relay(1)
-    down_send(3)
-    bd2.relay()
     hidden_tile(2, step, 0, 4)
-
-    def down_forward(k):
-        z = order[k]
-        done(ad2_last[k])
-        forward(fwd_d[k + 1], lambda c: a_d.at[c, :, z])
-        forward(fwd_d[k + 1], lambda c: b_d.at[c, z])
 
     got_r1, got_r2 = {}, {}
     own, back, ahead, opposite = range(N)
 
-    pairs = (pl.ds(0, 2), pl.ds(2, 2))
-    rounds = [
-        (order[0], xi, before, (xi, before)),
-        (order[0], after, far, (after, far)),
-        (order[1], *pairs, range(N)),
-        (order[2], *pairs, range(N)),
-        (order[3], 0, 1, (0, 1)),
-        (order[3], 2, 3, (2, 3)),
-    ]
+    order = [(0, 0), (0, 1), (1, 0), (2, 0), (0, 2), (1, 1), (1, 2), (2, 1), (2, 2), (0, 3), (3, 0),
+             (1, 3), (2, 3), (3, 1), (3, 2), (3, 3)]
+    blocks = [(places_z[i], places_x[j]) for i, j in order]
+    rounds = [(blocks[r], blocks[r + 1]) for r in range(0, len(blocks), 2)]
 
     def sum_first(r):
-        z, low, high, _ = rounds[r]
+        low, high = rounds[r]
         got_r1[r] = [
-            send_to("y", 1, parts.at[opposite, z, low], r1.at[0, z, low]),
-            send_to("y", -1, parts.at[opposite, z, high], r1.at[1, z, high]),
+            send_to("y", 1, parts.at[(opposite, *low)], r1.at[(0, *low)]),
+            send_to("y", -1, parts.at[(opposite, *high)], r1.at[(1, *high)]),
         ]
 
     def sum_direct(r):
-        z, low, high, _ = rounds[r]
+        low, high = rounds[r]
         got_r2[r] = [
-            send_to("y", 1, parts.at[ahead, z, high], r2.at[0, z, high]),
-            send_to("y", -1, parts.at[back, z, low], r2.at[1, z, low]),
+            send_to("y", 1, parts.at[(ahead, *high)], r2.at[(0, *high)]),
+            send_to("y", -1, parts.at[(back, *low)], r2.at[(1, *low)]),
         ]
 
     def send_to(axis, s, src, dst):
@@ -457,29 +467,23 @@
         return copy.wait_recv
 
     def sum_second(r):
-        z, low, high, _ = rounds[r]
-        got_r1[r][0]()
-        parts[ahead, z, low] = (
-            parts[ahead, z, low].astype(F32) + r1[0, z, low].astype(F32)
-        ).astype(BF)
-        got_r2[r].append(send_to("y", 1, parts.at[ahead, z, low], r2.at[0, z, low]))
-        got_r1[r][1]()
-        parts[back, z, high] = (
-            parts[back, z, high].astype(F32) + r1[1, z, high].astype(F32)
-        ).astype(BF)
-        got_r2[r].append(send_to("y", -1, parts.at[back, z, high], r2.at[1, z, high]))
+        for k, (s, rel, at) in enumerate(((1, ahead, rounds[r][0]), (-1, back, rounds[r][1]))):
+            got_r1[r][k]()
+            parts[(rel, *at)] = (
+                parts[(rel, *at)].astype(F32) + r1[(k, *at)].astype(F32)
+            ).astype(BF)
+            got_r2[r].append(send_to("y", s, parts.at[(rel, *at)], r2.at[(k, *at)]))
 
     def sum_last(r):
-        z, _, _, blocks = rounds[r]
         done(got_r2[r])
-        for x in blocks:
+        for z, x in rounds[r]:
             summed = (
                 parts[own, z, x].astype(F32) + r2[0, z, x].astype(F32) + r2[1, z, x].astype(F32)
             )
             cols = pl.ds(pl.multiple_of((z * N + x) * lane, lane), lane)
             out[:, cols] = (middle[:, cols].astype(F32) + summed).astype(BF)
 
-    def multiply(z, xs):
+    def multiply(r):
         weights = cat(
             [
                 cat(
@@ -491,7 +495,7 @@
                     ],
                     0,
                 )
-                for x in xs
+                for z, x in rounds[r]
             ],
             1,
         )
@@ -499,57 +503,69 @@
             rows_y = hidden[y * span : (y + 2) * span, :]
             result = jnp.dot(rows_y, weights, preferred_element_type=F32).astype(BF)
             for i in range(2):
-                for j, x in enumerate(xs):
+                for j, (z, x) in enumerate(rounds[r]):
                     parts[y + i, z, x] = result[
                         i * span : (i + 1) * span, j * lane : (j + 1) * lane
                     ]
 
     done(fwd_d[0])
-    multiply(order[0], (xi, before))
+    done(fwd_d[1])
+    multiply(0)
     sum_first(0)
+    multiply(1)
+    sum_first(1)
     sum_direct(0)
-    done(ad2_last[0])
-    forward(fwd_d[1], lambda c: a_d.at[c, wrap(xi, 2), zi])
-    down_relay(2)
-    bd2.near()
-    down_forward(1)
-    done(fwd_d[1])
-    multiply(order[0], (after, far))
-    sum_first(1)
     sum_direct(1)
-    sum_second(0)
+    down_near(1)
+    down_near_forward(2, 1)
+    down_near(2)
+    down_near_forward(3, 2)
     done(fwd_d[2])
-    multiply(order[1], (0, 1))
-    multiply(order[1], (2, 3))
+    multiply(2)
     sum_first(2)
     sum_direct(2)
-    down_relay(3)
-    down_forward(2)
+    down_far_forward(4, 0)
+    done(fwd_d[3])
+    multiply(3)
+    sum_first(3)
+    sum_second(0)
     sum_second(1)
-    done(fwd_d[3])
-    multiply(order[2], (0, 1))
-    multiply(order[2], (2, 3))
-    sum_first(3)
     sum_direct(3)
-    bd2.end()
-    down_forward(3)
+    done(fwd_d[4])
+    multiply(4)
+    sum_first(4)
+    down_near(3)
+    down_near_forward(5, 3)
     sum_second(2)
-    done(fwd_d[4])
-    multiply(order[3], (0, 1))
-    sum_first(4)
-    multiply(order[3], (2, 3))
+    sum_direct(4)
+    down_far_forward(6, 1)
+    down_far_forward(6, 2)
+    sum_second(3)
+    done(fwd_d[5])
+    done(fwd_d[6])
+    multiply(5)
     sum_first(5)
-    sum_direct(4)
+    multiply(6)
+    sum_first(6)
     sum_direct(5)
-    sum_second(3)
+    down_far_forward(7, 3)
+    sum_second(4)
+    done(fwd_d[7])
+    multiply(7)
+    sum_first(7)
+    sum_direct(6)
+    sum_direct(7)
     sum_last(0)
     sum_last(1)
-    sum_second(4)
     sum_second(5)
+    sum_second(6)
     sum_last(2)
     sum_last(3)
+    sum_second(7)
     sum_last(4)
     sum_last(5)
+    sum_last(6)
+    sum_last(7)
     assert len(sends) <= COPIES
     for copy in sends:
         copy.wait_send()
@@ -566,7 +582,7 @@
     anywhere = pl.BlockSpec(memory_space=pl.ANY)
     return pl.pallas_call(
         kernel,
-        out_shape=jax.ShapeDtypeStruct(tokens.shape, BF),
+        out_shape=pltpu.VMEM(tokens.shape, BF),
         in_specs=[anywhere] * 13,
         out_specs=pl.BlockSpec(memory_space=pltpu.VMEM),
         scratch_shapes=[

time: 91 us -> 86.9 us (0.955)
  Pallas kernels: 89 us -> 86 us
  local copies, waits for them, and re-layouts: 1.88 us -> 0.8 us
    pallas_call x1, Pallas kernels: 89 us -> 86 us  [per_device(): pl.pallas_call(kernel, out_shape=pltpu.VMEM(tokens.shape, BF), in_specs=[...]
    unnamed x1, local copies, waits for them, and re-layouts: 1.88 us -> 0.8 us
where the time goes in v4:
time: 86.9 us; the launch traced here: 86.8 us
  Pallas kernels  86 us (99%)
    pallas_call x1, Pallas kernels, per_device(): pl.pallas_call(kernel, out_shape=pltpu.VMEM(tokens.shape, BF), in_specs=[...  86 us

profile of v4, /device:TPU:1, one launch (start us, length us, event | category | flops | bytes accessed | tf_op | source)
XLA Modules:
  0.0 86.8 jit_solution(1705683978512131259)
XLA Ops:
  0.0 86.0 %shard_map.127 = bf16[128,2048]{1,0:T(8,128)(2,1)S(1)} custom-call(bf16[128,2048]{1,0:T(8,128)(2,1)} %tokens.1, bf16[64,128]{1,0:T(8,128)(2,1)} %bitcast.9, bf16[64,128]{1,0:T(8,128)(2,1)} %bitcast.10, bf16[64,128]{1,0:T(8,128)(2,1)} %bitcast.11, bf16[704,128]{1,0:T(8,128)(2,1)} %bitcast.6, bf16[704,128]{1,0:T(8,128)(2,1)} %bitcast.7, ...), custom_call_target="tpu_custom_call" | custom-call | tf_op jit(solution)/shard_map/pallas_call | solution.py:583
  86.0 0.8 copy.15

commit v5 on v4

--- a/solution.py
+++ b/solution.py
@@ -13,7 +13,7 @@
 TP = ("tp_0", "tp_1")
 EPS = 1e-06
 N = 4
-COPIES = 272
+COPIES = 280
 
 
 def row_waves(half):
@@ -258,6 +258,32 @@
     values = (
         (activated - center) * lax.rsqrt(spread + EPS) * row(lgain) + row(lshift)
     ).astype(BF)
+    done(fwd_g[:3])
+    ring_x = [xi, wrap(xi, -1), wrap(xi, 1), wrap(xi, 2)]
+
+    def gate_part(xs):
+        pairs = [(z, x) for z in range(N) for x in xs]
+        left = cat(
+            [nbuf[:, pl.ds(pl.multiple_of((z * N + x) * 128, 128), 128)] for z, x in pairs], 1
+        )
+        return cat(
+            [
+                dot_nt(
+                    left,
+                    cat(
+                        [
+                            cat([gw[c, x, z, y] for y in (lo, lo + 1) for c in range(2)], 0)
+                            for z, x in pairs
+                        ],
+                        1,
+                    ),
+                )
+                for lo in (0, 2)
+            ],
+            1,
+        )
+
+    gate_near = gate_part(ring_x[:3])
     finish_far(g3, fwd_g, group(gw), xi)
     finish_far(o3, fwd_o, group(ow), zi)
     span, groups = mixk.shape[1], mixk.shape[0]
@@ -272,8 +298,8 @@
             jnp.dot(masked, values[:, g * span : (g + 1) * span], preferred_element_type=F32)
             + offset
         )
-    done(fwd_g)
-    gate_u = gelu(cat([project(lambda c, y, z, x: gw[c, x, z, y], lo) for lo in (0, 2)], 1))
+    done(fwd_g[3:])
+    gate_u = gelu(gate_near + gate_part(ring_x[3:]))
     gated = (gate_u * cat(mixing, 1)).astype(BF)
     done(fwd_o)
     total = jnp.zeros((span, 1), F32)
@@ -348,17 +374,15 @@
 
     for ring in second[0]:
         ring.relay()
+    for ring in second[1]:
+        ring.relay()
+    second.append(wave_rings(2))
     done(own_d)
     ad1 = Ring("z", lambda i, h: a_d.at[ci, xi, i, pl.ds(h * hr, hr)])
     bd1 = Ring("x", lambda i, h: b_d.at[ci, zi, i, pl.ds(h * hr, hr)])
-    for ring in second[1]:
-        ring.relay()
-    second.append(wave_rings(2))
     near_wave(0)
     toks.relay()
     far_wave(0)
-    for ring in (ad1, bd1):
-        ring.relay()
     near_wave(1)
     toks.near()
     done(fwd_gu[0])
@@ -403,9 +427,9 @@
             gate_pre * lax.logistic(gate_pre) * up_pre
         ).astype(BF)
 
+    far_wave(1)
     hidden_tile(0, 0, 0, 3)
     hidden_tile(0, step, 0, 3)
-    far_wave(1)
     for ring in second[2]:
         ring.relay()
     down_send(0)
@@ -414,22 +438,22 @@
     hidden_tile(1, step, 0, 3)
     near_wave(2)
     for ring in (ad1, bd1):
+        ring.relay()
+    toks.end()
+    hidden_tile(0, 0, 3, 4)
+    hidden_tile(0, step, 3, 4)
+    for ring in (ad1, bd1):
         ring.near()
     down_send(1)
     down_send(2)
-    for ring in (ad1, bd1):
-        ring.end()
-    forward(fwd_d[0], lambda c: a_d.at[c, xi])
-    forward(fwd_d[0], lambda c: b_d.at[c, zi])
-    toks.end()
-    hidden_tile(0, 0, 3, 4)
-    hidden_tile(0, step, 3, 4)
+    for k in range(3):
+        forward(fwd_d[0], lambda c: block_a(c, xi, places_z[k]))
+        forward(fwd_d[0], lambda c: block_b(c, zi, places_x[k]))
     far_wave(2)
     hidden_tile(1, 0, 3, 4)
     hidden_tile(1, step, 3, 4)
     down_near(0)
     down_near_forward(1, 0)
-    down_send(3)
     done(fwd_gu[2])
     hidden_tile(2, 0, 0, 4)
     hidden_tile(2, step, 0, 4)
@@ -516,6 +540,11 @@
     sum_first(1)
     sum_direct(0)
     sum_direct(1)
+    for ring in (ad1, bd1):
+        ring.end()
+    down_send(3)
+    forward(fwd_d[4], lambda c: block_a(c, xi, places_z[3]))
+    forward(fwd_d[4], lambda c: block_b(c, zi, places_x[3]))
     down_near(1)
     down_near_forward(2, 1)
     down_near(2)
@@ -561,13 +590,16 @@
     sum_second(6)
     sum_last(2)
     sum_last(3)
+    early = len(sends) - 48
+    for copy in sends[:early]:
+        copy.wait_send()
     sum_second(7)
     sum_last(4)
     sum_last(5)
     sum_last(6)
     sum_last(7)
     assert len(sends) <= COPIES
-    for copy in sends:
+    for copy in sends[early:]:
         copy.wait_send()
 
 

time: 86.9 us -> 85.6 us (0.985)
  Pallas kernels: 86 us -> 84.8 us
    pallas_call x1, Pallas kernels: 86 us -> 84.8 us  [per_device(): pl.pallas_call(kernel, out_shape=pltpu.VMEM(tokens.shape, BF), in_specs=[...]
where the time goes in v5:
time: 85.6 us
  Pallas kernels  84.8 us (99%)
    pallas_call x1, Pallas kernels, per_device(): pl.pallas_call(kernel, out_shape=pltpu.VMEM(tokens.shape, BF), in_specs=[...  84.8 us

profile of v5, /device:TPU:1, one launch (start us, length us, event | category | flops | bytes accessed | tf_op | source)
XLA Modules:
  0.0 85.6 jit_solution(14712187387934405687)
XLA Ops:
  0.0 84.8 %shard_map.127 = bf16[128,2048]{1,0:T(8,128)(2,1)S(1)} custom-call(bf16[128,2048]{1,0:T(8,128)(2,1)} %tokens.1, bf16[64,128]{1,0:T(8,128)(2,1)} %bitcast.9, bf16[64,128]{1,0:T(8,128)(2,1)} %bitcast.10, bf16[64,128]{1,0:T(8,128)(2,1)} %bitcast.11, bf16[704,128]{1,0:T(8,128)(2,1)} %bitcast.6, bf16[704,128]{1,0:T(8,128)(2,1)} %bitcast.7, ...), custom_call_target="tpu_custom_call" | custom-call | tf_op jit(solution)/shard_map/pallas_call | solution.py:615
  84.8 0.8 copy.15

commit v6 on v5

--- a/solution.py
+++ b/solution.py
@@ -455,8 +455,8 @@
     down_near(0)
     down_near_forward(1, 0)
     done(fwd_gu[2])
-    hidden_tile(2, 0, 0, 4)
-    hidden_tile(2, step, 0, 4)
+    hidden_tile(2, 0, 1, 4)
+    hidden_tile(2, step, 1, 4)
 
     got_r1, got_r2 = {}, {}
     own, back, ahead, opposite = range(N)
@@ -507,7 +507,7 @@
             cols = pl.ds(pl.multiple_of((z * N + x) * lane, lane), lane)
             out[:, cols] = (middle[:, cols].astype(F32) + summed).astype(BF)
 
-    def multiply(r):
+    def multiply(r, pieces=((0, 2), (2, 4))):
         weights = cat(
             [
                 cat(
@@ -523,10 +523,10 @@
             ],
             1,
         )
-        for y in range(0, N, 2):
-            rows_y = hidden[y * span : (y + 2) * span, :]
+        for y, end in pieces:
+            rows_y = hidden[y * span : end * span, :]
             result = jnp.dot(rows_y, weights, preferred_element_type=F32).astype(BF)
-            for i in range(2):
+            for i in range(end - y):
                 for j, (z, x) in enumerate(rounds[r]):
                     parts[y + i, z, x] = result[
                         i * span : (i + 1) * span, j * lane : (j + 1) * lane
@@ -534,9 +534,10 @@
 
     done(fwd_d[0])
     done(fwd_d[1])
-    multiply(0)
+    sent = ((1, 2), (2, 4))
+    multiply(0, sent)
     sum_first(0)
-    multiply(1)
+    multiply(1, sent)
     sum_first(1)
     sum_direct(0)
     sum_direct(1)
@@ -549,6 +550,8 @@
     down_near_forward(2, 1)
     down_near(2)
     down_near_forward(3, 2)
+    hidden_tile(2, 0, 0, 1)
+    hidden_tile(2, step, 0, 1)
     done(fwd_d[2])
     multiply(2)
     sum_first(2)
@@ -584,6 +587,8 @@
     sum_first(7)
     sum_direct(6)
     sum_direct(7)
+    multiply(0, ((0, 1),))
+    multiply(1, ((0, 1),))
     sum_last(0)
     sum_last(1)
     sum_second(5)

time: 85.6 us -> 86.5 us (1.011)
    pallas_call x1, Pallas kernels: 84.8 us -> 85.6 us  [per_device(): pl.pallas_call(kernel, out_shape=pltpu.VMEM(tokens.shape, BF), in_specs=[...]
where the time goes in v6:
time: 86.5 us; the launch traced here: 86.4 us
  Pallas kernels  85.6 us (99%)
    pallas_call x1, Pallas kernels, per_device(): pl.pallas_call(kernel, out_shape=pltpu.VMEM(tokens.shape, BF), in_specs=[...  85.6 us

profile of v6, /device:TPU:1, one launch (start us, length us, event | category | flops | bytes accessed | tf_op | source)
XLA Modules:
  0.0 86.4 jit_solution(17256221193479565588)
XLA Ops:
  0.0 85.6 %shard_map.127 = bf16[128,2048]{1,0:T(8,128)(2,1)S(1)} custom-call(bf16[128,2048]{1,0:T(8,128)(2,1)} %tokens.1, bf16[64,128]{1,0:T(8,128)(2,1)} %bitcast.9, bf16[64,128]{1,0:T(8,128)(2,1)} %bitcast.10, bf16[64,128]{1,0:T(8,128)(2,1)} %bitcast.11, bf16[704,128]{1,0:T(8,128)(2,1)} %bitcast.6, bf16[704,128]{1,0:T(8,128)(2,1)} %bitcast.7, ...), custom_call_target="tpu_custom_call" | custom-call | tf_op jit(solution)/shard_map/pallas_call | solution.py:620
  85.6 0.8 copy.15
